TPU v7x, 32 devices: a whole 2x2x4 slice. The times are simulated.
32 devices in a mesh: sp: 8 (over z, x), tp: 4 (over y, core).
Axes of the slice: x: 2, y: 2, z: 4, core: 2. Of those that a mesh axis runs over, the one named last changes fastest.
Arguments:
- tokens: bfloat16 [768, 1024], P(('sp', 'tp')), may hold values from -11 to 11, as said below
- doc_ids: int32 [768], P('sp'), may hold values from 0 to 1, never falling along the last dimension, each value on 1 to 576 neighbouring positions
- query_down: bfloat16 [1024, 384], P('sp'), may hold values from -0.1875 to 0.1875
- query_gain: float32 [384], replicated, may hold values from 0.1 to 1.9
- query_up: bfloat16 [384, 16, 96], P('sp', 'tp'), may hold values from -0.3125 to 0.3125
- latent_down: bfloat16 [1024, 256], P('sp'), may hold values from -0.1875 to 0.1875
- latent_gain: float32 [256], replicated, may hold values from 0.1 to 1.9
- rope_down: bfloat16 [1024, 32], P('sp'), may hold values from -0.1875 to 0.1875
- key_up: bfloat16 [256, 16, 64], P('sp', 'tp'), may hold values from -0.375 to 0.375
- value_up: bfloat16 [256, 16, 64], P('sp', 'tp'), may hold values from -0.375 to 0.375
- output_weight: bfloat16 [1024, 1024], P('tp', 'sp'), may hold values from -0.1875 to 0.1875
- output_gain: float32 [1024], replicated, may hold values from 0.1 to 1.9
Outputs:
- layer_out: bfloat16 [768, 1024], P(('sp', 'tp'))
Inputs may be any that keep to these rules, and one draw needn't show every extreme that they name: Every entry of tokens lies between -11 and 11. `doc_ids`: document numbers never fall along the sequence; each document holds 1 to 576 positions.
All inputs are finite; a program needn't handle non-finite values.
Results may differ from a plain program's by a relative error of at most 0.02.
Values may be sent and summed in bfloat16 or wider, within the bound.
A program may use at most 64 MiB of HBM per device.

v0:
```python
import jax
import jax.numpy as jnp
from jax import lax
from jax.sharding import PartitionSpec as P

ROPE_BASE = 10000.0
EPS = 1e-06
MASKED = -1e30


def folded(value, axis, dim, update, carry):
    whole = jax.tree.map(lambda part: lax.all_gather(part, axis, axis=dim, tiled=True), value)
    return update(carry, whole, jnp.int32(0))


def gathered_then(share, axis, dim, apply):
    everything = lax.all_gather(share, axis, axis=dim, tiled=True)
    return apply(everything, jnp.int32(0))


def for_sending(value):
    def short(part):
        return part.astype(jnp.bfloat16) if part.dtype == jnp.float32 else part

    return jax.tree.map(short, value)


def own_rows(term, extent, axis):
    whole = term(jnp.int32(0), extent * lax.axis_size(axis)).astype(jnp.bfloat16)
    return lax.psum_scatter(whole, axis, scatter_dimension=0, tiled=True).astype(jnp.float32)


def normalize(values, gain_vec):
    return values * lax.rsqrt(jnp.mean(values * values, axis=-1, keepdims=True) + EPS) * gain_vec


def rotate(rope_part, position):
    half_width = rope_part.shape[-1] // 2
    frequency = ROPE_BASE ** (
        -jnp.arange(0, 2 * half_width, 2, dtype=jnp.float32) / (2 * half_width)
    )
    angles = position.astype(jnp.float32)[:, None] * frequency[None, :]
    cosine = jnp.cos(angles)
    sine_part = jnp.sin(angles)
    if rope_part.ndim == 3:
        cosine = cosine[:, None, :]
        sine_part = sine_part[:, None, :]
    first_half = rope_part[..., :half_width]
    second_half = rope_part[..., half_width:]
    return jnp.concatenate(
        [
            first_half * cosine - second_half * sine_part,
            first_half * sine_part + second_half * cosine,
        ],
        axis=-1,
    )


def on_device(
    tokens,
    doc_ids,
    query_down,
    query_gain,
    query_up,
    latent_down,
    latent_gain,
    rope_down,
    key_up,
    value_up,
    output_weight,
    output_gain,
):
    row_count = tokens.shape[0]
    key_span = doc_ids.shape[0]
    query_width = query_down.shape[1]
    latent_width = latent_down.shape[1]
    rope_width = rope_down.shape[1]
    local_heads = query_up.shape[1]
    head_width = query_up.shape[2]
    nope_width = key_up.shape[2]
    value_width = value_up.shape[2]

    def down_term(total_now, weight_rows, first_row):
        columns = lax.dynamic_slice_in_dim(tokens, first_row, weight_rows.shape[0], 1)
        return total_now + jnp.dot(columns, weight_rows, preferred_element_type=jnp.float32)

    empty_query = jnp.zeros((row_count, query_width), jnp.float32)
    empty_latent = jnp.zeros((row_count, latent_width), jnp.float32)
    empty_rope = jnp.zeros((row_count, rope_width), jnp.float32)
    query_sum = folded(query_down, "sp", 0, down_term, empty_query)
    latent_sum = folded(latent_down, "sp", 0, down_term, empty_latent)
    rope_sum = folded(rope_down, "sp", 0, down_term, empty_rope)
    query_lat = normalize(query_sum, query_gain).astype(jnp.bfloat16)
    kv_lat = normalize(latent_sum, latent_gain).astype(jnp.bfloat16)
    own_position = lax.axis_index(("sp", "tp")) * row_count + lax.iota(jnp.int32, row_count)
    rope_keys = rotate(rope_sum, own_position).astype(jnp.bfloat16)
    query_full, key_full, value_full = (
        lax.all_gather(query_up, "sp", axis=0, tiled=True),
        lax.all_gather(key_up, "sp", axis=0, tiled=True),
        lax.all_gather(value_up, "sp", axis=0, tiled=True),
    )
    flat_width = local_heads * head_width
    query_matrix = query_full.reshape(query_width, flat_width)
    block_offset = lax.axis_index("sp") * key_span

    def project(latent_rows, first_row):
        piece_rows = latent_rows.shape[0]
        raw_query = jnp.dot(
            latent_rows[:, :query_width], query_matrix, preferred_element_type=jnp.float32
        ).reshape(piece_rows, local_heads, head_width)
        position = block_offset + first_row + lax.iota(jnp.int32, piece_rows)
        turned = jnp.concatenate(
            [raw_query[..., :nope_width], rotate(raw_query[..., nope_width:], position)], axis=-1
        )
        return jnp.concatenate(
            [
                turned.astype(jnp.bfloat16).reshape(piece_rows, flat_width),
                latent_rows[:, query_width:],
            ],
            axis=1,
        )

    packed = jnp.concatenate([query_lat, kv_lat, rope_keys], axis=1)
    gathered = gathered_then(packed, "tp", 0, project)
    queries = gathered[:, :flat_width].reshape(key_span, local_heads, head_width)
    my_ids = doc_ids.astype(jnp.bfloat16)
    key_rows = jnp.concatenate([gathered[:, flat_width:], my_ids[:, None]], axis=1)
    query_nope = queries[..., :nope_width]
    query_rope = queries[..., nope_width:]
    score_scale = head_width ** (-0.5)
    absorbed = jnp.einsum("qhe,rhe->qhr", query_nope, key_full, preferred_element_type=jnp.float32)

    def block_scores(latent_part, rope_part):
        latent_float = latent_part.astype(jnp.float32)
        scores = jnp.einsum("qhr,kr->qhk", absorbed, latent_float, precision=lax.Precision.HIGHEST)
        scores = scores + jnp.einsum(
            "qhe,ke->qhk", query_rope, rope_part, preferred_element_type=jnp.float32
        )
        return (scores * score_scale, latent_float)

    def finish(averaged):
        return jnp.einsum(
            "qhr,rhv->qhv",
            averaged,
            value_full.astype(jnp.float32),
            precision=lax.Precision.HIGHEST,
        )

    def scan_step(state_now, block_keys):
        row_peak, row_total, running = state_now
        latent_part = block_keys[:, :latent_width]
        rope_part = block_keys[:, latent_width : latent_width + rope_width]
        block_ids = block_keys[:, latent_width + rope_width]
        scores, value_part = block_scores(latent_part, rope_part)
        same_doc = my_ids[:, None, None] == block_ids[None, None, :]
        peak_new = jnp.maximum(row_peak, jnp.max(jnp.where(same_doc, scores, MASKED), axis=-1))
        soft_weights = jnp.where(same_doc, jnp.exp(scores - peak_new[..., None]), 0.0)
        factor = jnp.exp(row_peak - peak_new)
        if value_part.ndim == 3:
            contrib = jnp.einsum(
                "qhk,khv->qhv", soft_weights, value_part, precision=lax.Precision.HIGHEST
            )
        else:
            contrib = jnp.einsum(
                "qhk,kv->qhv", soft_weights, value_part, precision=lax.Precision.HIGHEST
            )
        next_state = (
            peak_new,
            row_total * factor + jnp.sum(soft_weights, axis=-1),
            running * factor[..., None] + contrib,
        )
        return (next_state, None)

    def fold_keys(state_now, key_piece, first_row):
        key_blocks = key_piece.reshape(key_piece.shape[0] // key_span, key_span, key_piece.shape[1])
        return lax.scan(scan_step, state_now, key_blocks)[0]

    start_state = (
        jnp.full((key_span, local_heads), MASKED, jnp.float32),
        jnp.zeros((key_span, local_heads), jnp.float32),
        jnp.zeros((key_span, local_heads, latent_width), jnp.float32),
    )
    row_peak, row_total, running = folded(for_sending(key_rows), "sp", 0, fold_keys, start_state)
    averaged = running / row_total[..., None]
    attended = finish(averaged).astype(jnp.bfloat16).reshape(key_span, local_heads * value_width)
    out_full = lax.all_gather(output_weight, "sp", axis=1, tiled=True)

    def out_term(first_row, row_span):
        row_block = lax.dynamic_slice_in_dim(attended, first_row, row_span, 0)
        return jnp.dot(row_block, out_full, preferred_element_type=jnp.float32)

    mixed = own_rows(out_term, row_count, "tp")
    return normalize(mixed, output_gain).astype(jnp.bfloat16)


def solution(mesh):
    in_specs = (
        P(("sp", "tp"), None),
        P("sp"),
        P("sp", None),
        P(),
        P("sp", "tp", None),
        P("sp", None),
        P(),
        P("sp", None),
        P("sp", "tp", None),
        P("sp", "tp", None),
        P("tp", "sp"),
        P(),
    )
    out_specs = P(("sp", "tp"), None)
    return jax.shard_map(
        on_device, mesh=mesh, in_specs=in_specs, out_specs=out_specs, check_vma=False
    )
```

profile of v0, /device:TPU:0, one launch (start us, length us, event | category | flops | bytes accessed | tf_op | source)
XLA Modules:
  0.0 311.1 jit_solution(12510070031708650458)
XLA Ops:
  6.6 32.6 %all_gather.29 = bf16[1024,32]{0,1:T(8,128)(2,1)S(1)} all-gather(bf16[128,32]{0,1:T(8,128)(2,1)} %param.21), channel_id=1, replica_groups=mesh['sp'=8,'tp'=4] {'sp'}, dimensions={0}, use_global_device_ids=true | all-gather | bytes 73728 | tf_op jit(solution)/shard_map/all_gather | solution.py:12
  39.2 32.1 %all_gather.27 = bf16[1024,384]{1,0:T(8,128)(2,1)S(1)} all-gather(bf16[128,384]{1,0:T(8,128)(2,1)S(1)} %copy-done.3), channel_id=1, replica_groups=mesh['sp'=8,'tp'=4] {'sp'}, dimensions={0}, use_global_device_ids=true | all-gather | bytes 884736 | tf_op jit(solution)/shard_map/all_gather | solution.py:12
  71.8 0.5 copy-done.4
  72.3 31.2 %all_gather.28 = bf16[1024,256]{1,0:T(8,128)(2,1)S(1)} all-gather(bf16[128,256]{1,0:T(8,128)(2,1)S(1)} %copy-done.4), channel_id=1, replica_groups=mesh['sp'=8,'tp'=4] {'sp'}, dimensions={0}, use_global_device_ids=true | all-gather | bytes 589824 | tf_op jit(solution)/shard_map/all_gather | solution.py:12
  103.9 0.5 copy-done.10
  104.6 0.7 copy-done.11
  105.4 5.6 %all_gather.30 = bf16[96,672]{1,0:T(8,128)(2,1)S(1)} all-gather(bf16[24,672]{1,0:T(8,128)(2,1)S(1)} %pad_maximum_fusion.1), channel_id=1, replica_groups=mesh['sp'=8,'tp'=4] {'tp'}, dimensions={0}, use_global_device_ids=true | all-gather | bytes 161280 | tf_op jit(solution)/shard_map/all_gather | solution.py:17
  111.0 31.1 %all_gather.32 = bf16[384,4,96]{2,1,0:T(4,128)(2,1)S(1)} all-gather(bf16[48,4,96]{2,1,0:T(4,128)(2,1)S(1)} %copy-done.6), channel_id=1, replica_groups=mesh['sp'=8,'tp'=4] {'sp'}, dimensions={0}, use_global_device_ids=true | all-gather | bytes 331776 | tf_op jit(solution)/shard_map/all_gather | solution.py:98
  143.1 31.0 %all_gather.33 = bf16[256,4,64]{2,0,1:T(8,128)(2,1)S(1)} all-gather(bf16[32,4,64]{2,0,1:T(8,128)(2,1)S(1)} %copy.29), channel_id=1, replica_groups=mesh['sp'=8,'tp'=4] {'sp'}, dimensions={0}, use_global_device_ids=true | all-gather | bytes 147456 | tf_op jit(solution)/shard_map/all_gather | solution.py:99
  174.4 31.4 %all_gather.31 = bf16[768,289]{1,0:T(8,128)(2,1)S(1)} all-gather(bf16[96,289]{1,0:T(8,128)(2,1)S(1)} %pad_maximum_fusion), channel_id=1, replica_groups=mesh['sp'=8,'tp'=4] {'sp'}, dimensions={0}, use_global_device_ids=true | all-gather | bytes 499392 | tf_op jit(solution)/shard_map/all_gather | solution.py:12
  206.1 11.6 %while.15 = (s32[]{:T(128)}, f32[96,4]{0,1:T(4,128)S(1)}, f32[96,4]{0,1:T(4,128)S(1)}, f32[96,4,256]{2,0,1:T(8,128)S(1)}, bf16[96]{0:T(256)(128)(2,1)S(1)}, /*in...) while((s32[]{:T(128)}, f32[96,4]{0,1:T(4,128)S(1)}, ...), condition=%wide.region_5.6_spmd.clone, body=%wide.region_2.5_spmd.clone.sunk | while | flops 229489536 | bytes 2351349 | solution.py:176
  207.1 0.5 convolution_add_fusion.3
  208.0 0.4 select_reduce_fusion.2
  208.6 0.5 convolution_add_fusion.3
  209.5 0.4 select_reduce_fusion.2
  210.0 0.5 convolution_add_fusion.3
  210.9 0.4 select_reduce_fusion.2
  211.5 0.5 convolution_add_fusion.3
  212.4 0.4 select_reduce_fusion.2
  212.9 0.5 convolution_add_fusion.3
  213.8 0.4 select_reduce_fusion.2
  214.4 0.5 convolution_add_fusion.3
  215.3 0.4 select_reduce_fusion.2
  215.8 0.5 convolution_add_fusion.3
  217.3 0.5 convolution_add_fusion.3
  217.8 31.0 %all_gather.34 = bf16[256,4,64]{2,0,1:T(8,128)(2,1)S(1)} all-gather(bf16[32,4,64]{2,0,1:T(8,128)(2,1)S(1)} %copy.30), channel_id=1, replica_groups=mesh['sp'=8,'tp'=4] {'sp'}, dimensions={0}, use_global_device_ids=true | all-gather | bytes 147456 | tf_op jit(solution)/shard_map/all_gather | solution.py:100
  248.8 31.6 %all_gather.35 = bf16[256,1024]{1,0:T(8,128)(2,1)S(1)} all-gather(bf16[256,128]{1,0:T(8,128)(2,1)S(1)} %copy-done.5), channel_id=1, replica_groups=mesh['sp'=8,'tp'=4] {'sp'}, dimensions={1}, use_global_device_ids=true | all-gather | bytes 589824 | tf_op jit(solution)/shard_map/all_gather | solution.py:186
  280.4 0.5 convolution_convert_fusion.1
  280.9 0.9 convolution_convert_fusion
  281.8 20.7 %reduce-scatter.2.cloned.1.call-done = bf16[24,1024]{1,0:T(8,128)(2,1)} async-done(((bf16[96,1024]{1,0:T(8,128)(2,1)}), bf16[24,1024]{1,0:T(8,128)(2,1)}) %reduce-scatter.2.cloned.1.call-update) | async-done | bytes 49168 | tf_op jit(solution)/shard_map/reduce_scatter | solution.py:30
  302.6 1.0 fusion.13
  303.6 0.7 fusion.15
  (120 shorter events, 7.7 us)
Async XLA Ops:
  6.5 64.8 %copy-start = (bf16[24,1024]{1,0:T(8,128)(2,1)S(1)}, bf16[24,1024]{1,0:T(8,128)(2,1)}, u32[]{:S(2)}) copy-start(bf16[24,1024]{1,0:T(8,128)(2,1)} %param.14) | copy-start | bytes 147460
  6.5 32.7 %copy-start.3 = (bf16[128,384]{1,0:T(8,128)(2,1)S(1)}, bf16[128,384]{1,0:T(8,128)(2,1)}, u32[]{:S(2)}) copy-start(bf16[128,384]{1,0:T(8,128)(2,1)} %param.16) | copy-start | bytes 294916
  6.5 296.0 %reduce-scatter.2.cloned.1.call-start = ((), (), s32[]{:S(2)}) async-start(), calls=%async_computation.1 | async-start | bytes 245760 | tf_op jit(solution)/shard_map/reduce_scatter | solution.py:30
  71.5 0.9 copy-start.4
  103.8 0.7 copy-start.10
  104.6 0.7 copy-start.11
  105.4 5.6 %copy-start.6 = (bf16[48,4,96]{2,1,0:T(4,128)(2,1)S(1)}, bf16[48,4,96]{2,1,0:T(4,128)(2,1)}, u32[]{:S(2)}) copy-start(bf16[48,4,96]{2,1,0:T(4,128)(2,1)} %param.18) | copy-start | bytes 110596
  111.0 31.3 %copy-start.1 = (bf16[96,672]{1,0:T(8,128)(2,1)}, bf16[96,672]{1,0:T(8,128)(2,1)S(1)}, u32[]{:S(2)}) copy-start(bf16[96,672]{1,0:T(8,128)(2,1)S(1)} %all_gather.30) | copy-start | bytes 387076
  142.3 0.8 copy-start.7
  143.1 31.1 %copy-start.12 = (s32[96]{0:T(128)S(1)}, s32[96]{0:T(128)}, u32[]{:S(2)}) copy-start(s32[96]{0:T(128)} %param.15) | copy-start | bytes 1156
  143.1 31.2 %slice-start = ((bf16[96,672]{1,0:T(8,128)(2,1)}), bf16[96,288]{1,0:T(8,128)(2,1)S(1)}, s32[]{:S(2)}) async-start(bf16[96,672]{1,0:T(8,128)(2,1)} %copy-done.1), calls=%async_computation.2 | async-start | bytes 147456 | tf_op jit(solution)/shard_map/slice | solution.py:118
  206.1 11.6 %copy-start.8 = (bf16[32,4,64]{2,1,0:T(4,128)(2,1)S(1)}, bf16[32,4,64]{2,1,0:T(4,128)(2,1)}, u32[]{:S(2)}) copy-start(bf16[32,4,64]{2,1,0:T(4,128)(2,1)} %param.23) | copy-start | bytes 49156
  217.8 31.1 %copy-start.5 = (bf16[256,128]{1,0:T(8,128)(2,1)S(1)}, bf16[256,128]{1,0:T(8,128)(2,1)}, u32[]{:S(2)}) copy-start(bf16[256,128]{1,0:T(8,128)(2,1)} %param.24) | copy-start | bytes 196612
  281.8 21.8 %copy-start.9 = (f32[1024]{0:T(1024)S(1)}, f32[1024]{0:T(1024)}, u32[]{:S(2)}) copy-start(f32[1024]{0:T(1024)} %param.25) | copy-start | bytes 12292
  302.6 1.0 copy-start.2
Sparse Core Ops, SparseCore 0:
  281.9 20.5 reduce-scatter.1
where the time goes:
time: 312 us; the launch traced here: 311 us
  blocking collectives  258 us (83%)
  waiting for transfers between devices  20.8 us (7%)
  between operations  13.6 us (4%)
  matrix products  10.7 us (3%)
  local copies, waits for them, and re-layouts  4.08 us (1%)
  other arithmetic  3.78 us (1%)
    all_gather x4, blocking collectives, folded(): lax.all_gather(part, axis, axis=dim, tiled=True)  127 us
    all_gather x1, blocking collectives, on_device(): out_full = lax.all_gather(output_weight, 'sp', axis=1, tiled=True)  31.6 us
    all_gather x1, blocking collectives, on_device(): lax.all_gather(query_up, 'sp', axis=0, tiled=True)  31.1 us
    all_gather x1, blocking collectives, on_device(): lax.all_gather(key_up, 'sp', axis=0, tiled=True)  31 us
    all_gather x1, blocking collectives, on_device(): lax.all_gather(value_up, 'sp', axis=0, tiled=True)  31 us
    reduce_scatter x1, waiting for transfers between devices, own_rows(): lax.psum_scatter(whole, axis, scatter_dimension=0, tiled=True)  20.7 us
  transfers between devices with their start and end apart: 1, of which 1 were waited for; matrix products, arithmetic and copies ran while one was open for 0% of the time, Pallas kernels for 0%

commit v1 on v0

--- a/solution.py
+++ b/solution.py
@@ -1,6 +1,11 @@
+import functools
+
 import jax
 import jax.numpy as jnp
+import numpy as np
 from jax import lax
+from jax.experimental import pallas as pl
+from jax.experimental.pallas import tpu as pltpu
 from jax.sharding import PartitionSpec as P
 
 ROPE_BASE = 10000.0
@@ -56,7 +61,7 @@
     )
 
 
-def on_device(
+def plain_layer(
     tokens,
     doc_ids,
     query_down,
@@ -193,6 +198,342 @@
     return normalize(mixed, output_gain).astype(jnp.bfloat16)
 
 
+MESH = pl.DeviceIdType.MESH
+LANES = 128
+PENALTY = 1e6
+
+
+def nt_dot(left, right):
+    return lax.dot_general(
+        left, right, (((1,), (1,)), ((), ())), preferred_element_type=jnp.float32
+    )
+
+
+def nn_dot(left, right):
+    return jnp.dot(left, right, preferred_element_type=jnp.float32)
+
+
+def layer_kernel(
+    sizes,
+    tok,
+    ids,
+    down,
+    query_up,
+    kv_up,
+    out_w,
+    query_gain,
+    latent_gain,
+    output_gain,
+    table,
+    out,
+    tok_all,
+    down_all,
+    query_all,
+    kvup_all,
+    out_all,
+    raw_all,
+    row_buf,
+    row_all,
+    part_buf,
+    part_all,
+    table_buf,
+    weight_send,
+    weight_recv,
+    row_send,
+    row_recv,
+    tok_send,
+    tok_recv,
+    raw_send,
+    raw_recv,
+    part_send,
+    part_recv,
+    local_sem,
+):
+    S, T, H, N, V, R = (sizes[k] for k in ("S", "T", "H", "N", "V", "R"))
+    QW, LW = sizes["QW"], sizes["LW"]
+    rows = tok.shape[0]
+    span = rows * T
+    half = S // 2
+    s = lax.axis_index("sp")
+    t = lax.axis_index("tp")
+    pair = s + 1 - 2 * (s % 2)
+
+    def line(k):
+        return (s + 2 * k) % S
+
+    def mate(k):
+        return (t + k) % T
+
+    table_copy = pltpu.make_async_copy(
+        table.at[:, pl.ds(pl.multiple_of(s * span, 8), span)], table_buf, local_sem.at[0]
+    )
+    table_copy.start()
+
+    barrier = pltpu.get_barrier_semaphore()
+    for k in range(1, half):
+        pl.semaphore_signal(barrier, inc=1, device_id={"sp": line(k), "tp": t}, device_id_type=MESH)
+    pl.semaphore_signal(barrier, inc=1, device_id={"sp": pair, "tp": t}, device_id_type=MESH)
+    for k in range(1, T):
+        pl.semaphore_signal(barrier, inc=1, device_id={"sp": s, "tp": mate(k)}, device_id_type=MESH)
+    pl.semaphore_wait(barrier, half - 1 + 1 + T - 1)
+
+    def spread(own, whole, send, recv, where):
+        sent = []
+        for k in range(1, half):
+            copy = pltpu.make_async_remote_copy(
+                src_ref=own, dst_ref=whole.at[s], send_sem=send.at[where(k - 1)],
+                recv_sem=recv.at[where(k - 1)], device_id={"sp": line(k), "tp": t},
+                device_id_type=MESH)
+            copy.start()
+            sent.append(copy)
+        copy = pltpu.make_async_remote_copy(
+            src_ref=own, dst_ref=whole.at[s], send_sem=send.at[where(half - 1)],
+            recv_sem=recv.at[where(half - 1)], device_id={"sp": pair, "tp": t},
+            device_id_type=MESH)
+        copy.start()
+        sent.append(copy)
+        return sent
+
+    def arrival(own, whole, send, recv, slot):
+        return pltpu.make_async_remote_copy(
+            src_ref=own, dst_ref=whole.at[s], send_sem=send, recv_sem=recv,
+            device_id={"sp": pair, "tp": t}, device_id_type=MESH)
+
+    def pass_on(own, whole, send, recv, where, sent, k):
+        arrival(own, whole, send.at[where(k - 1)], recv.at[where(k - 1)], k).wait_recv()
+        block = line(half - k)
+        copy = pltpu.make_async_remote_copy(
+            src_ref=whole.at[block], dst_ref=whole.at[block],
+            send_sem=send.at[where(half - 1 + k)], recv_sem=recv.at[where(half - 1 + k)],
+            device_id={"sp": pair, "tp": t}, device_id_type=MESH)
+        copy.start()
+        sent.append(copy)
+        return block
+
+    def from_pair(own, whole, send, recv, where, j):
+        arrival(own, whole, send.at[where(half - 1 + j)], recv.at[where(half - 1 + j)], j).wait_recv()
+        return (pair + 2 * (half - j)) % S
+
+    def to_mates(src_of, dst, send, recv):
+        sent = []
+        for k in range(1, T):
+            copy = pltpu.make_async_remote_copy(
+                src_ref=src_of(k), dst_ref=dst, send_sem=send.at[k - 1], recv_sem=recv.at[k - 1],
+                device_id={"sp": s, "tp": mate(k)}, device_id_type=MESH)
+            copy.start()
+            sent.append(copy)
+        return sent
+
+    tok_sent = to_mates(lambda k: tok, tok_all.at[t], tok_send, tok_recv)
+    arrays = [(down, down_all), (query_up, query_all), (kv_up, kvup_all), (out_w, out_all)]
+    sends = [weight_send.at[i] for i in range(4)]
+    recvs = [weight_recv.at[i] for i in range(4)]
+    same = lambda i: i
+    weight_sent = [spread(own, whole, sends[i], recvs[i], same) for i, (own, whole) in enumerate(arrays)]
+    tok_all[t] = tok[...]
+    for own, whole in arrays:
+        whole[s] = own[...]
+
+    def relay(i):
+        own, whole = arrays[i]
+        for k in range(1, half):
+            pass_on(own, whole, sends[i], recvs[i], same, weight_sent[i], k)
+
+    def rest(i):
+        own, whole = arrays[i]
+        for j in range(half):
+            from_pair(own, whole, sends[i], recvs[i], same, j)
+
+    relay(0)
+    for copy in tok_sent:
+        copy.wait_recv()
+    rest(0)
+    block_tokens = tok_all[...].astype(jnp.float32).reshape(span, tok.shape[1]).astype(jnp.bfloat16)
+    depth = down.shape[1]
+    raw = nt_dot(block_tokens[:, :depth], down_all[0])
+    for j in range(1, S):
+        raw = raw + nt_dot(block_tokens[:, j * depth:(j + 1) * depth], down_all[j])
+    raw_all[t] = raw.astype(jnp.bfloat16)
+    raw_sent = to_mates(lambda k: raw_all.at[t], raw_all.at[t], raw_send, raw_recv)
+    relay(1)
+    relay(2)
+    table_copy.wait()
+    for copy in raw_sent:
+        copy.wait_recv()
+    whole_raw = jnp.concatenate([raw_all[j].astype(jnp.float32) for j in range(T)], axis=1)
+    query_raw = whole_raw[:, :QW]
+    rope_raw = whole_raw[:, QW:QW + LANES]
+    latent_raw = whole_raw[:, QW + LANES:QW + LANES + LW]
+    cosine = table_buf[0]
+    sine = table_buf[1]
+    lane = lax.broadcasted_iota(jnp.int32, (span, LANES), 1)
+    own_id = ids[...]
+    h2 = R // 2
+    id_lane = lane - h2
+    is_id = (lane >= h2) & (lane < LANES // 2)
+
+    def turn(x):
+        return x * cosine + pltpu.roll(x, LANES // 2, 1) * sine
+
+    key_rope = turn(rope_raw)
+    key_marks = jnp.where(is_id & (id_lane != own_id), -1.0, 0.0)
+    row_buf[:, :LW] = normalize(latent_raw, latent_gain[...]).astype(jnp.bfloat16)
+    row_buf[:, LW:] = jnp.where(is_id, key_marks, key_rope).astype(jnp.bfloat16)
+    row_sent = spread(row_buf, row_all, row_send, row_recv, same)
+    row_all[s] = row_buf[...]
+
+    query_lat = normalize(query_raw, query_gain[...]).astype(jnp.bfloat16)
+    rest(1)
+    queries = nn_dot(query_lat, query_all[...].reshape(QW, query_up.shape[1]))
+    nope = queries[:, :H * N].astype(jnp.bfloat16)
+    rope = turn(queries[:, H * N:])
+    nope_lane = lax.broadcasted_iota(jnp.int32, (span, H * N), 1)
+    spread_nope = jnp.concatenate(
+        [jnp.where((nope_lane >= h * N) & (nope_lane < (h + 1) * N), nope, jnp.zeros_like(nope)) for h in range(H)],
+        axis=0)
+    is_rope = (lane < h2) | ((lane >= LANES // 2) & (lane < LANES // 2 + h2))
+    query_marks = jnp.where(is_id & (id_lane == own_id), PENALTY, 0.0)
+    spread_rope = jnp.concatenate(
+        [jnp.where(is_rope, rope if h == 0 else pltpu.roll(rope, LANES - h * h2, 1), query_marks).astype(jnp.bfloat16) for h in range(H)],
+        axis=0)
+    rest(2)
+    rank_rows = kv_up.shape[0] // 2
+    key_matrix = kvup_all[:, :rank_rows, :].reshape(LW, kv_up.shape[1])
+    value_matrix = kvup_all[:, rank_rows:, :].reshape(LW, kv_up.shape[1])
+    absorbed = nt_dot(spread_nope, key_matrix).astype(jnp.bfloat16)
+    for k in range(1, half):
+        pass_on(row_buf, row_all, row_send, row_recv, same, row_sent, k)
+    relay(3)
+    for j in range(half):
+        from_pair(row_buf, row_all, row_send, row_recv, same, j)
+    key_rows = row_all[...].reshape(S * span, LW + LANES)
+    latent_rows = key_rows[:, :LW]
+    scores = nt_dot(absorbed, latent_rows) + nt_dot(spread_rope, key_rows[:, LW:])
+    scores = scores * ((N + R) ** (-0.5))
+    weights = jnp.exp(scores - jnp.max(scores, axis=-1, keepdims=True))
+    total = jnp.sum(weights, axis=-1, keepdims=True)
+    averaged = nn_dot(weights.astype(jnp.bfloat16), latent_rows) / total
+    everything = nn_dot(averaged.astype(jnp.bfloat16), value_matrix)
+    value_lane = lax.broadcasted_iota(jnp.int32, (span, H * V), 1)
+    attended = jnp.zeros((span, H * V), jnp.float32)
+    for h in range(H):
+        attended = jnp.where(
+            (value_lane >= h * V) & (value_lane < (h + 1) * V), everything[h * span:(h + 1) * span], attended)
+    attended = attended.astype(jnp.bfloat16)
+    rest(3)
+    columns = out_w.shape[1]
+    for j in range(S):
+        part = nn_dot(attended, out_all[j])
+        for i in range(T):
+            part_buf[i, :, j * columns:(j + 1) * columns] = part[i * rows:(i + 1) * rows].astype(jnp.bfloat16)
+    part_sent = []
+    for k in range(1, T):
+        copy = pltpu.make_async_remote_copy(
+            src_ref=part_buf.at[mate(k)], dst_ref=part_all.at[k - 1], send_sem=part_send.at[k - 1],
+            recv_sem=part_recv.at[k - 1], device_id={"sp": s, "tp": mate(k)}, device_id_type=MESH)
+        copy.start()
+        part_sent.append(copy)
+    mixed = part_buf[t].astype(jnp.float32)
+    for k in range(1, T):
+        part_sent[k - 1].wait_recv()
+        mixed = mixed + part_all[k - 1].astype(jnp.float32)
+    out[...] = normalize(mixed, output_gain[...]).astype(jnp.bfloat16)
+    for copy in tok_sent + raw_sent + row_sent + part_sent + [c for group in weight_sent for c in group]:
+        copy.wait_send()
+
+
+def kernel_fits(mesh, tokens, query_down, query_up, latent_down, rope_down, key_up, value_up, output_weight):
+    S, T = mesh.shape["sp"], mesh.shape["tp"]
+    H, N, V, R = query_up.shape[1], key_up.shape[2], value_up.shape[2], rope_down.shape[1]
+    columns = query_down.shape[1] + latent_down.shape[1] + LANES
+    return (
+        S % 2 == 0 and S >= 4
+        and tokens.shape[0] % 8 == 0
+        and query_down.shape[0] % LANES == 0
+        and query_down.shape[1] % LANES == 0
+        and latent_down.shape[1] % LANES == 0
+        and columns % (16 * T) == 0
+        and query_up.shape[0] % 16 == 0
+        and key_up.shape[0] % 16 == 0
+        and output_weight.shape[1] % LANES == 0
+        and H * R == LANES
+        and H * N % LANES == 0
+        and N == V
+    )
+
+
+def rope_tables(positions, width, copies):
+    h2 = width // 2
+    frequency = ROPE_BASE ** (-np.arange(0, width, 2, dtype=np.float64) / width)
+    angles = np.arange(positions, dtype=np.float64)[:, None] * frequency[None, :]
+    cosine = np.tile(np.cos(angles), (1, 2 * copies))
+    sine = np.tile(np.sin(angles), (1, copies))
+    return np.stack([cosine, np.concatenate([-sine, sine], axis=1)]).astype(np.float32)
+
+
+def on_device(mesh, tokens, doc_ids, query_down, query_gain, query_up, latent_down, latent_gain,
+              rope_down, key_up, value_up, output_weight, output_gain):
+    if not kernel_fits(mesh, tokens, query_down, query_up, latent_down, rope_down, key_up, value_up, output_weight):
+        return plain_layer(tokens, doc_ids, query_down, query_gain, query_up, latent_down, latent_gain,
+                           rope_down, key_up, value_up, output_weight, output_gain)
+    S, T = mesh.shape["sp"], mesh.shape["tp"]
+    H, N, V, R = query_up.shape[1], key_up.shape[2], value_up.shape[2], rope_down.shape[1]
+    QW, LW = query_down.shape[1], latent_down.shape[1]
+    rows, width = tokens.shape
+    span = rows * T
+    h2 = R // 2
+    depth = query_down.shape[0]
+    gap = jnp.zeros((depth, LANES // 2 - h2), jnp.bfloat16)
+    packed = jnp.concatenate(
+        [query_down, rope_down[:, :h2], gap, rope_down[:, h2:], gap, latent_down], axis=1)
+    share = packed.shape[1] // T
+    down = lax.dynamic_slice_in_dim(packed, lax.axis_index("tp") * share, share, 1).T
+    q_rows = query_up.shape[0]
+    query_pack = jnp.concatenate(
+        [query_up[..., :N].reshape(q_rows, H * N),
+         query_up[..., N:].reshape(q_rows, H, 2, h2).transpose(0, 2, 1, 3).reshape(q_rows, H * R)], axis=1)
+    k_rows = key_up.shape[0]
+    kv_pack = jnp.concatenate([key_up.reshape(k_rows, H * N), value_up.reshape(k_rows, H * V)], axis=0)
+    table = jnp.asarray(rope_tables(S * span, R, H))
+    sizes = dict(S=S, T=T, H=H, N=N, V=V, R=R, QW=QW, LW=LW)
+    vmem = pl.BlockSpec(memory_space=pltpu.VMEM)
+    bf16 = jnp.bfloat16
+    sem = pltpu.SemaphoreType.DMA
+    return pl.pallas_call(
+        functools.partial(layer_kernel, sizes),
+        out_shape=jax.ShapeDtypeStruct((rows, width), bf16),
+        in_specs=[vmem] * 9 + [pl.BlockSpec(memory_space=pl.ANY)],
+        out_specs=vmem,
+        scratch_shapes=[
+            pltpu.VMEM((T, rows, width), bf16),
+            pltpu.VMEM((S,) + down.shape, bf16),
+            pltpu.VMEM((S,) + query_pack.shape, bf16),
+            pltpu.VMEM((S,) + kv_pack.shape, bf16),
+            pltpu.VMEM((S,) + output_weight.shape, bf16),
+            pltpu.VMEM((T, span, share), bf16),
+            pltpu.VMEM((span, LW + LANES), bf16),
+            pltpu.VMEM((S, span, LW + LANES), bf16),
+            pltpu.VMEM((T, rows, width), bf16),
+            pltpu.VMEM((T - 1, rows, width), bf16),
+            pltpu.VMEM((2, span, LANES), jnp.float32),
+            sem((4, S - 1)),
+            sem((4, S - 1)),
+            sem((S - 1,)),
+            sem((S - 1,)),
+            sem((T - 1,)),
+            sem((T - 1,)),
+            sem((T - 1,)),
+            sem((T - 1,)),
+            sem((T - 1,)),
+            sem((T - 1,)),
+            sem((1,)),
+        ],
+        compiler_params=pltpu.CompilerParams(
+            collective_id=0, has_side_effects=True, vmem_limit_bytes=48 * 1024 * 1024),
+    )(tokens, doc_ids[:, None], down, query_pack, kv_pack, output_weight,
+      query_gain[None, :], latent_gain[None, :], output_gain[None, :], table)
+
+
 def solution(mesh):
     in_specs = (
         P(("sp", "tp"), None),
@@ -210,5 +551,5 @@
     )
     out_specs = P(("sp", "tp"), None)
     return jax.shard_map(
-        on_device, mesh=mesh, in_specs=in_specs, out_specs=out_specs, check_vma=False
-    )
+        functools.partial(on_device, mesh), mesh=mesh, in_specs=in_specs, out_specs=out_specs, check_vma=False
+    )

time: 312 us -> 53 us (0.17)
  blocking collectives: 258 us -> 0 us
  Pallas kernels: 0 us -> 42.8 us
  waiting for transfers between devices: 20.8 us -> 0 us
  between operations: 13.6 us -> 0.12 us
  matrix products: 10.7 us -> 0 us
  local copies, waits for them, and re-layouts: 4.08 us -> 9.47 us
  other arithmetic: 3.78 us -> 0.01 us
    all_gather x9 -> x0, blocking collectives: 258 us -> none  [the longest x4 127 us: folded(): lax.all_gather(part, axis, axis=dim, tiled=True)]
    pallas_call x0 -> x1, Pallas kernels: none -> 42.8 us  [on_device(): pl.pallas_call(functools.partial(layer_kernel, sizes), out_shape=jax.Shap...]
    reduce_scatter x1 -> x0, waiting for transfers between devices: 20.7 us -> none  [own_rows(): lax.psum_scatter(whole, axis, scatter_dimension=0, tiled=True)]
    dot_general x31 -> x0, matrix products: 10.7 us -> none  [the longest x8 3.64 us: scan_step(): jnp.einsum('qhk,kv->qhv', soft_weights, value_part, precision=lax.Precisi...]
    unnamed x28 -> x29, local copies, waits for them, and re-layouts: 2.16 us -> 8.05 us
  transfers between devices with their start and end apart: 1 -> 0, of which waited for: 1 -> 0; matrix products, arithmetic and copies ran while one was open for 0% -> 0% of each run, Pallas kernels for 0% -> 0%
where the time goes in v1:
time: 53 us; the launch traced here: 52.4 us
  Pallas kernels  42.8 us (81%)
  local copies, waits for them, and re-layouts  9.47 us (18%)
    pallas_call x1, Pallas kernels, on_device(): pl.pallas_call(functools.partial(layer_kernel, sizes), out_shape=jax.Shap...  42.8 us
    unnamed x29, local copies, waits for them, and re-layouts  8.05 us

profile of v1, /device:TPU:0, one launch (start us, length us, event | category | flops | bytes accessed | tf_op | source)
XLA Modules:
  0.0 52.4 jit_solution(16518056054545630672)
XLA Ops:
  0.0 0.0 copy-start
  0.0 1.1 %copy.18 = bf16[128,384]{0,1:T(8,128)(2,1)S(1)} copy(bf16[128,384]{1,0:T(8,128)(2,1)} %param.15) | data formatting | bytes 196608 | tf_op args[2]
  1.1 0.7 %constant_dynamic-update-slice_fusion.4 = bf16[128,768]{0,1:T(8,128)(2,1)S(1)} fusion(bf16[128,768]{0,1:T(8,128)(2,1)S(1)} %constant_dynamic-update-slice_fusion.5, bf16[128,32]{0,1:T(8,128)(2,1)} %param.20), kind=kLoop, calls=%fused_computation.7 | loop fusion | bytes 8192
  1.8 0.7 %constant_dynamic-update-slice_fusion.2 = bf16[128,768]{0,1:T(8,128)(2,1)S(1)} fusion(bf16[128,768]{0,1:T(8,128)(2,1)S(1)} %constant_dynamic-update-slice_fusion.3, bf16[128,32]{0,1:T(8,128)(2,1)} %param.20), kind=kLoop, calls=%fused_computation.5 | loop fusion | bytes 8192
  2.5 0.9 %copy.19 = bf16[128,256]{0,1:T(8,128)(2,1)S(1)} copy(bf16[128,256]{1,0:T(8,128)(2,1)} %param.18) | data formatting | bytes 131072 | tf_op args[5]
  3.5 0.9 %slice.15 = bf16[48,4,32]{2,1,0:T(4,128)(2,1)S(1)} slice(bf16[48,4,96]{2,1,0:T(4,128)(2,1)} %param.17), slice={[0:48], [0:4], [64:96]} | slice | bytes 24576 | tf_op jit(solution)/shard_map/slice | solution.py:494
  4.4 0.1 copy.24
  4.5 0.0 copy-start.5
  4.5 0.1 copy.22
  4.6 0.7 %copy-done.5 = bf16[48,4,96]{2,1,0:T(4,128)(2,1)S(1)} copy-done((bf16[48,4,96]{2,1,0:T(4,128)(2,1)S(1)}, bf16[48,4,96]{2,1,0:T(4,128)(2,1)}, u32[]{:S(2)}) %copy-start.5) | copy-done | bytes 36888
  5.3 0.1 reshape.15
  5.4 0.0 copy-start.6
  5.4 0.7 %copy-done.6 = bf16[32,4,64]{2,1,0:T(4,128)(2,1)S(1)} copy-done((bf16[32,4,64]{2,1,0:T(4,128)(2,1)S(1)}, bf16[32,4,64]{2,1,0:T(4,128)(2,1)}, u32[]{:S(2)}) %copy-start.6) | copy-done | bytes 16408
  6.2 0.0 copy-start.7
  6.2 0.1 reshape.18
  6.3 0.7 %copy-done.7 = bf16[32,4,64]{2,1,0:T(4,128)(2,1)S(1)} copy-done((bf16[32,4,64]{2,1,0:T(4,128)(2,1)S(1)}, bf16[32,4,64]{2,1,0:T(4,128)(2,1)}, u32[]{:S(2)}) %copy-start.7) | copy-done | bytes 16408
  6.9 0.0 copy-start.9
  6.9 0.1 reshape.19
  7.0 0.0 copy-start.1
  7.0 0.0 copy-start.2
  7.1 0.5 %copy-done.9 = s32[96]{0:T(128)S(1)} copy-done((s32[96]{0:T(128)S(1)}, s32[96]{0:T(128)}, u32[]{:S(2)}) %copy-start.9) | copy-done | bytes 408
  7.6 0.0 copy-start.8
  7.6 0.1 copy.23.ids
  7.7 0.6 %copy-done.8 = f32[384]{0:T(512)S(1)} copy-done((f32[384]{0:T(512)S(1)}, f32[384]{0:T(512)}, u32[]{:S(2)}) %copy-start.8) | copy-done | bytes 1560
  8.3 0.0 copy-start.4
  8.3 0.0 copy-done
  8.3 0.0 copy-done.1
  8.3 0.0 copy-done.2
  8.3 0.7 %copy-done.3 = f32[1024]{0:T(1024)S(1)} copy-done((f32[1024]{0:T(1024)S(1)}, f32[1024]{0:T(1024)}, u32[]{:S(2)}) %copy-start.3) | copy-done | bytes 4120
  9.0 0.0 copy-done.4
  9.0 42.8 %shard_map.127 = bf16[24,1024]{1,0:T(8,128)(2,1)S(1)} custom-call(bf16[24,1024]{1,0:T(8,128)(2,1)S(1)} %copy-done.2, s32[96,1]{1,0:T(8,128)S(1)} %copy.23.ids, bf16[192,128]{1,0:T(8,128)(2,1)S(1)} %dynamic-slice_bitcast_fusion.down, bf16[48,384]{1,0:T(8,128)(2,1)S(1)} %pad_maximum_fusion.query_up, bf16[64,256]{1,0:T(8,128)(2,1)S(1)} %pad_maximum_fusion.1.kv_up, ...), custom_call_target="tpu_custom_call" | custom-call | tf_op jit(solution)/shard_map/pallas_call | solution.py:502
  51.8 0.6 %copy.31 = bf16[24,1024]{1,0:T(8,128)(2,1)} copy(bf16[24,1024]{1,0:T(8,128)(2,1)S(1)} %shard_map.127) | data formatting | bytes 98304
  (10 shorter events, 0.1 us)
Async XLA Ops:
  0.0 8.3 %copy-start = (f32[2,768,128]{2,1,0:T(8,128)S(1)}, f32[2,768,128]{2,1,0:T(8,128)}, u32[]{:S(2)}) copy-start(f32[2,768,128]{2,1,0:T(8,128)} %constant.14.clone.table) | copy-start | bytes 2359300
  4.5 0.8 %copy-start.5 = (bf16[48,4,96]{2,1,0:T(4,128)(2,1)S(1)}, bf16[48,4,96]{2,1,0:T(4,128)(2,1)}, u32[]{:S(2)}) copy-start(bf16[48,4,96]{2,1,0:T(4,128)(2,1)} %param.17) | copy-start | bytes 110596
  5.4 0.8 %copy-start.6 = (bf16[32,4,64]{2,1,0:T(4,128)(2,1)S(1)}, bf16[32,4,64]{2,1,0:T(4,128)(2,1)}, u32[]{:S(2)}) copy-start(bf16[32,4,64]{2,1,0:T(4,128)(2,1)} %param.21) | copy-start | bytes 49156
  6.2 0.8 %copy-start.7 = (bf16[32,4,64]{2,1,0:T(4,128)(2,1)S(1)}, bf16[32,4,64]{2,1,0:T(4,128)(2,1)}, u32[]{:S(2)}) copy-start(bf16[32,4,64]{2,1,0:T(4,128)(2,1)} %param.22) | copy-start | bytes 49156
  6.9 0.7 %copy-start.9 = (s32[96]{0:T(128)S(1)}, s32[96]{0:T(128)}, u32[]{:S(2)}) copy-start(s32[96]{0:T(128)} %param.14) | copy-start | bytes 1156
  7.0 1.2 %copy-start.1 = (bf16[256,128]{1,0:T(8,128)(2,1)S(1)}, bf16[256,128]{1,0:T(8,128)(2,1)}, u32[]{:S(2)}) copy-start(bf16[256,128]{1,0:T(8,128)(2,1)} %out_w.1) | copy-start | bytes 196612
  7.0 1.3 %copy-start.2 = (bf16[24,1024]{1,0:T(8,128)(2,1)S(1)}, bf16[24,1024]{1,0:T(8,128)(2,1)}, u32[]{:S(2)}) copy-start(bf16[24,1024]{1,0:T(8,128)(2,1)} %tok.1) | copy-start | bytes 147460
  7.6 0.7 %copy-start.8 = (f32[384]{0:T(512)S(1)}, f32[384]{0:T(512)}, u32[]{:S(2)}) copy-start(f32[384]{0:T(512)} %param.16) | copy-start | bytes 4612
  8.3 0.7 %copy-start.3 = (f32[1024]{0:T(1024)S(1)}, f32[1024]{0:T(1024)}, u32[]{:S(2)}) copy-start(f32[1024]{0:T(1024)} %param.24) | copy-start | bytes 12292
  8.3 0.7 %copy-start.4 = (f32[256]{0:T(256)S(1)}, f32[256]{0:T(256)}, u32[]{:S(2)}) copy-start(f32[256]{0:T(256)} %param.19) | copy-start | bytes 3076

commit v2 on v1

--- a/solution.py
+++ b/solution.py
@@ -215,18 +215,38 @@
 
 def layer_kernel(
     sizes,
-    tok,
+    tok_in,
+    ids_in,
+    query_down,
+    latent_down,
+    rope_down,
+    query_up,
+    key_up,
+    value_up,
+    out_in,
+    query_gain_in,
+    latent_gain_in,
+    output_gain_in,
+    table,
+    out,
     ids,
-    down,
-    query_up,
-    kv_up,
-    out_w,
     query_gain,
     latent_gain,
     output_gain,
-    table,
-    out,
+    tok,
+    query_down_buf,
+    latent_down_buf,
+    rope_down_buf,
+    query_up_buf,
+    key_up_buf,
+    value_up_buf,
+    out_w,
+    table_buf,
+    pack,
+    query_pack,
+    kv_pack,
     tok_all,
+    tok_flat,
     down_all,
     query_all,
     kvup_all,
@@ -236,11 +256,12 @@
     row_all,
     part_buf,
     part_all,
-    table_buf,
     weight_send,
     weight_recv,
     row_send,
     row_recv,
+    core_send,
+    core_recv,
     tok_send,
     tok_recv,
     raw_send,
@@ -251,12 +272,17 @@
 ):
     S, T, H, N, V, R = (sizes[k] for k in ("S", "T", "H", "N", "V", "R"))
     QW, LW = sizes["QW"], sizes["LW"]
+    f32, bf16 = jnp.float32, jnp.bfloat16
     rows = tok.shape[0]
     span = rows * T
     half = S // 2
+    h2 = R // 2
+    depth = query_down.shape[0]
+    share = down_all.shape[1]
     s = lax.axis_index("sp")
     t = lax.axis_index("tp")
     pair = s + 1 - 2 * (s % 2)
+    twin = t + 1 - 2 * (t % 2)
 
     def line(k):
         return (s + 2 * k) % S
@@ -264,10 +290,10 @@
     def mate(k):
         return (t + k) % T
 
-    table_copy = pltpu.make_async_copy(
-        table.at[:, pl.ds(pl.multiple_of(s * span, 8), span)], table_buf, local_sem.at[0]
-    )
-    table_copy.start()
+    def remote(src, dst, send, recv, sp, tp):
+        return pltpu.make_async_remote_copy(
+            src_ref=src, dst_ref=dst, send_sem=send, recv_sem=recv,
+            device_id={"sp": sp, "tp": tp}, device_id_type=MESH)
 
     barrier = pltpu.get_barrier_semaphore()
     for k in range(1, half):
@@ -275,117 +301,163 @@
     pl.semaphore_signal(barrier, inc=1, device_id={"sp": pair, "tp": t}, device_id_type=MESH)
     for k in range(1, T):
         pl.semaphore_signal(barrier, inc=1, device_id={"sp": s, "tp": mate(k)}, device_id_type=MESH)
+
+    loads = [
+        (query_down, query_down_buf),
+        (latent_down, latent_down_buf),
+        (rope_down, rope_down_buf),
+        (tok_in, tok),
+        (query_up, query_up_buf),
+        (key_up, key_up_buf),
+        (value_up, value_up_buf),
+        (out_in, out_w),
+        (table.at[:, pl.ds(pl.multiple_of(s * span, 8), span)], table_buf),
+        (ids_in, ids),
+        (query_gain_in, query_gain),
+        (latent_gain_in, latent_gain),
+        (output_gain_in, output_gain),
+    ]
+    copies = []
+    for i, (src, dst) in enumerate(loads):
+        copy = pltpu.make_async_copy(src, dst, local_sem.at[i])
+        copy.start()
+        copies.append(copy)
+
+    for copy in copies[:3]:
+        copy.wait()
+    pack[:QW] = query_down_buf[...].astype(f32).T.astype(bf16)
+    pack[QW + LANES:] = latent_down_buf[...].astype(f32).T.astype(bf16)
+    rope_cols = rope_down_buf[...].astype(f32)
+    gap = jnp.zeros((LANES // 2 - h2, depth), f32)
+    pack[QW:QW + LANES] = jnp.concatenate(
+        [rope_cols[:h2], gap, rope_cols[h2:R], gap], axis=0).astype(bf16)
+    down = pack.at[pl.ds(pl.multiple_of(t * share, 16), share)]
+    copies[3].wait()
     pl.semaphore_wait(barrier, half - 1 + 1 + T - 1)
 
-    def spread(own, whole, send, recv, where):
+    def spread(own, view, send, recv):
         sent = []
         for k in range(1, half):
-            copy = pltpu.make_async_remote_copy(
-                src_ref=own, dst_ref=whole.at[s], send_sem=send.at[where(k - 1)],
-                recv_sem=recv.at[where(k - 1)], device_id={"sp": line(k), "tp": t},
-                device_id_type=MESH)
+            sent.append(remote(own, view(s), send.at[k - 1], recv.at[k - 1], line(k), t))
+        sent.append(remote(own, view(s), send.at[half - 1], recv.at[half - 1], pair, t))
+        for copy in sent:
             copy.start()
-            sent.append(copy)
-        copy = pltpu.make_async_remote_copy(
-            src_ref=own, dst_ref=whole.at[s], send_sem=send.at[where(half - 1)],
-            recv_sem=recv.at[where(half - 1)], device_id={"sp": pair, "tp": t},
-            device_id_type=MESH)
-        copy.start()
-        sent.append(copy)
         return sent
 
-    def arrival(own, whole, send, recv, slot):
-        return pltpu.make_async_remote_copy(
-            src_ref=own, dst_ref=whole.at[s], send_sem=send, recv_sem=recv,
-            device_id={"sp": pair, "tp": t}, device_id_type=MESH)
-
-    def pass_on(own, whole, send, recv, where, sent, k):
-        arrival(own, whole, send.at[where(k - 1)], recv.at[where(k - 1)], k).wait_recv()
+    def landed(view, send, recv, slot):
+        remote(view(s), view(s), send.at[slot], recv.at[slot], pair, t).wait_recv()
+
+    def pass_on(view, send, recv, sent, k):
+        landed(view, send, recv, k - 1)
         block = line(half - k)
-        copy = pltpu.make_async_remote_copy(
-            src_ref=whole.at[block], dst_ref=whole.at[block],
-            send_sem=send.at[where(half - 1 + k)], recv_sem=recv.at[where(half - 1 + k)],
-            device_id={"sp": pair, "tp": t}, device_id_type=MESH)
+        slot = half - 1 + k
+        copy = remote(view(block), view(block), send.at[slot], recv.at[slot], pair, t)
         copy.start()
         sent.append(copy)
         return block
 
-    def from_pair(own, whole, send, recv, where, j):
-        arrival(own, whole, send.at[where(half - 1 + j)], recv.at[where(half - 1 + j)], j).wait_recv()
+    def pair_block(j):
         return (pair + 2 * (half - j)) % S
 
     def to_mates(src_of, dst, send, recv):
-        sent = []
-        for k in range(1, T):
-            copy = pltpu.make_async_remote_copy(
-                src_ref=src_of(k), dst_ref=dst, send_sem=send.at[k - 1], recv_sem=recv.at[k - 1],
-                device_id={"sp": s, "tp": mate(k)}, device_id_type=MESH)
+        sent = [remote(src_of(k), dst, send.at[k - 1], recv.at[k - 1], s, mate(k)) for k in range(1, T)]
+        for copy in sent:
             copy.start()
-            sent.append(copy)
         return sent
 
+    wholes = [down_all, query_all, kvup_all, out_all]
+    owns = [down, query_pack, kv_pack, out_w]
+    views = [lambda i, w=w: w.at[i] for w in wholes]
+    weight_sent = [[], [], [], []]
+
+    def begin(i):
+        weight_sent[i] += spread(owns[i], views[i], weight_send.at[i], weight_recv.at[i])
+
+    def relay(i, then=None):
+        for k in range(1, half):
+            block = pass_on(views[i], weight_send.at[i], weight_recv.at[i], weight_sent[i], k)
+            if then is not None:
+                then(block)
+
+    def rest(i, then=None):
+        for j in range(half):
+            landed(views[i], weight_send.at[i], weight_recv.at[i], half - 1 + j)
+            if then is not None:
+                then(pair_block(j))
+
+    begin(0)
     tok_sent = to_mates(lambda k: tok, tok_all.at[t], tok_send, tok_recv)
-    arrays = [(down, down_all), (query_up, query_all), (kv_up, kvup_all), (out_w, out_all)]
-    sends = [weight_send.at[i] for i in range(4)]
-    recvs = [weight_recv.at[i] for i in range(4)]
-    same = lambda i: i
-    weight_sent = [spread(own, whole, sends[i], recvs[i], same) for i, (own, whole) in enumerate(arrays)]
+    down_all[s] = down[...]
     tok_all[t] = tok[...]
-    for own, whole in arrays:
-        whole[s] = own[...]
-
-    def relay(i):
-        own, whole = arrays[i]
-        for k in range(1, half):
-            pass_on(own, whole, sends[i], recvs[i], same, weight_sent[i], k)
-
-    def rest(i):
-        own, whole = arrays[i]
-        for j in range(half):
-            from_pair(own, whole, sends[i], recvs[i], same, j)
-
-    relay(0)
+
+    for copy in copies[4:8]:
+        copy.wait()
+    query_in = [query_up_buf[:, h, :].astype(f32) for h in range(H)]
+    query_pack[...] = jnp.concatenate(
+        [x[:, :N] for x in query_in] + [x[:, N:N + h2] for x in query_in] + [x[:, N + h2:] for x in query_in],
+        axis=1).astype(bf16)
+    k_rows = key_up.shape[0]
+    kv_pack[:k_rows] = jnp.concatenate([key_up_buf[:, h, :].astype(f32) for h in range(H)], axis=1).astype(bf16)
+    kv_pack[k_rows:] = jnp.concatenate([value_up_buf[:, h, :].astype(f32) for h in range(H)], axis=1).astype(bf16)
+    query_all[s] = query_pack[...]
+    kvup_all[s] = kv_pack[...]
+    out_all[s] = out_w[...]
+
     for copy in tok_sent:
         copy.wait_recv()
-    rest(0)
-    block_tokens = tok_all[...].astype(jnp.float32).reshape(span, tok.shape[1]).astype(jnp.bfloat16)
-    depth = down.shape[1]
-    raw = nt_dot(block_tokens[:, :depth], down_all[0])
-    for j in range(1, S):
-        raw = raw + nt_dot(block_tokens[:, j * depth:(j + 1) * depth], down_all[j])
-    raw_all[t] = raw.astype(jnp.bfloat16)
+    tok_flat[...] = tok_all[...].astype(f32).reshape(span, tok.shape[1]).astype(bf16)
+    total_raw = [jnp.zeros((span, share), f32)]
+
+    def down_block(block):
+        columns = tok_flat[:, pl.ds(pl.multiple_of(block * depth, LANES), depth)]
+        total_raw[0] = total_raw[0] + nt_dot(columns, down_all[block])
+
+    down_block(s)
+    relay(0, down_block)
+    begin(1)
+    begin(2)
+    rest(0, down_block)
+    raw_all[t] = total_raw[0].astype(bf16)
     raw_sent = to_mates(lambda k: raw_all.at[t], raw_all.at[t], raw_send, raw_recv)
-    relay(1)
-    relay(2)
-    table_copy.wait()
+    for copy in copies[8:]:
+        copy.wait()
+    cosine = table_buf[0]
+    sine = table_buf[1]
+    lane = lax.broadcasted_iota(jnp.int32, (span, LANES), 1)
+    padded = -(-span // LANES) * LANES
+    id_row = jnp.concatenate([ids[...].astype(f32), jnp.zeros((1, padded - span), f32)], axis=1)
+    own_id = jnp.broadcast_to(id_row, (LANES, padded)).T[:span]
+    id_lane = (lane - h2).astype(f32)
+    is_id = (lane >= h2) & (lane < LANES // 2)
+
     for copy in raw_sent:
         copy.wait_recv()
-    whole_raw = jnp.concatenate([raw_all[j].astype(jnp.float32) for j in range(T)], axis=1)
+    whole_raw = jnp.concatenate([raw_all[j].astype(f32) for j in range(T)], axis=1)
     query_raw = whole_raw[:, :QW]
     rope_raw = whole_raw[:, QW:QW + LANES]
     latent_raw = whole_raw[:, QW + LANES:QW + LANES + LW]
-    cosine = table_buf[0]
-    sine = table_buf[1]
-    lane = lax.broadcasted_iota(jnp.int32, (span, LANES), 1)
-    own_id = ids[...]
-    h2 = R // 2
-    id_lane = lane - h2
-    is_id = (lane >= h2) & (lane < LANES // 2)
 
     def turn(x):
         return x * cosine + pltpu.roll(x, LANES // 2, 1) * sine
 
-    key_rope = turn(rope_raw)
     key_marks = jnp.where(is_id & (id_lane != own_id), -1.0, 0.0)
-    row_buf[:, :LW] = normalize(latent_raw, latent_gain[...]).astype(jnp.bfloat16)
-    row_buf[:, LW:] = jnp.where(is_id, key_marks, key_rope).astype(jnp.bfloat16)
-    row_sent = spread(row_buf, row_all, row_send, row_recv, same)
-    row_all[s] = row_buf[...]
-
-    query_lat = normalize(query_raw, query_gain[...]).astype(jnp.bfloat16)
+    row_buf[:, :LW] = normalize(latent_raw, latent_gain[...]).astype(bf16)
+    row_buf[:, LW:] = jnp.where(is_id, key_marks, turn(rope_raw)).astype(bf16)
+    part_rows = span // 2
+    mine = pl.ds(pl.multiple_of((t % 2) * part_rows, 16), part_rows)
+
+    def row_view(i):
+        return row_all.at[i, mine]
+
+    row_sent = spread(row_buf.at[mine], row_view, row_send, row_recv)
+    relay(1)
+    relay(2)
+    begin(3)
+
+    query_lat = normalize(query_raw, query_gain[...]).astype(bf16)
     rest(1)
-    queries = nn_dot(query_lat, query_all[...].reshape(QW, query_up.shape[1]))
-    nope = queries[:, :H * N].astype(jnp.bfloat16)
+    queries = nn_dot(query_lat, query_all[...].reshape(QW, query_pack.shape[1]))
+    nope = queries[:, :H * N].astype(bf16)
     rope = turn(queries[:, H * N:])
     nope_lane = lax.broadcasted_iota(jnp.int32, (span, H * N), 1)
     spread_nope = jnp.concatenate(
@@ -394,51 +466,79 @@
     is_rope = (lane < h2) | ((lane >= LANES // 2) & (lane < LANES // 2 + h2))
     query_marks = jnp.where(is_id & (id_lane == own_id), PENALTY, 0.0)
     spread_rope = jnp.concatenate(
-        [jnp.where(is_rope, rope if h == 0 else pltpu.roll(rope, LANES - h * h2, 1), query_marks).astype(jnp.bfloat16) for h in range(H)],
+        [jnp.where(is_rope, rope if h == 0 else pltpu.roll(rope, LANES - h * h2, 1), query_marks).astype(bf16) for h in range(H)],
         axis=0)
+    core_sent = []
+
+    def to_twin(block, slot):
+        copy = remote(row_view(block), row_view(block), core_send.at[slot], core_recv.at[slot], s, twin)
+        copy.start()
+        core_sent.append(copy)
+
     rest(2)
-    rank_rows = kv_up.shape[0] // 2
-    key_matrix = kvup_all[:, :rank_rows, :].reshape(LW, kv_up.shape[1])
-    value_matrix = kvup_all[:, rank_rows:, :].reshape(LW, kv_up.shape[1])
-    absorbed = nt_dot(spread_nope, key_matrix).astype(jnp.bfloat16)
-    for k in range(1, half):
-        pass_on(row_buf, row_all, row_send, row_recv, same, row_sent, k)
+    key_matrix = kvup_all[:, :k_rows, :].reshape(LW, kv_pack.shape[1])
+    value_matrix = kvup_all[:, k_rows:, :].reshape(LW, kv_pack.shape[1])
+    absorbed = nt_dot(spread_nope, key_matrix).astype(bf16)
+    wide_query = jnp.concatenate([absorbed, spread_rope], axis=1)
+    scale = (N + R) ** (-0.5)
+
+    def block_scores(key_rows):
+        return nt_dot(wide_query, key_rows) * scale
+
+    first = block_scores(row_buf[...])
+    peak = jnp.max(first, axis=-1, keepdims=True)
+    first = jnp.exp(first - peak)
+    state = [peak, jnp.sum(first, axis=-1, keepdims=True), nn_dot(first.astype(bf16), row_buf[:, :LW])]
+
+    def fold(blocks):
+        key_rows = jnp.concatenate([row_all[b].astype(f32) for b in blocks], axis=0).astype(bf16)
+        scores = block_scores(key_rows)
+        peak, total, running = state
+        peak_new = jnp.maximum(peak, jnp.max(scores, axis=-1, keepdims=True))
+        factor = jnp.exp(peak - peak_new)
+        weights = jnp.exp(scores - peak_new)
+        state[0] = peak_new
+        state[1] = total * factor + jnp.sum(weights, axis=-1, keepdims=True)
+        state[2] = running * factor + nn_dot(weights.astype(bf16), key_rows[:, :LW])
+
+    blocks = [pass_on(row_view, row_send, row_recv, row_sent, k) for k in range(1, half)]
+    for slot, block in enumerate(blocks):
+        to_twin(block, slot)
+    for j in range(half):
+        landed(row_view, row_send, row_recv, half - 1 + j)
+        to_twin(pair_block(j), half - 1 + j)
+    for copy in core_sent[:half - 1]:
+        copy.wait_recv()
+    fold(blocks)
+    for copy in core_sent[half - 1:]:
+        copy.wait_recv()
+    fold([pair_block(j) for j in range(half)])
     relay(3)
-    for j in range(half):
-        from_pair(row_buf, row_all, row_send, row_recv, same, j)
-    key_rows = row_all[...].reshape(S * span, LW + LANES)
-    latent_rows = key_rows[:, :LW]
-    scores = nt_dot(absorbed, latent_rows) + nt_dot(spread_rope, key_rows[:, LW:])
-    scores = scores * ((N + R) ** (-0.5))
-    weights = jnp.exp(scores - jnp.max(scores, axis=-1, keepdims=True))
-    total = jnp.sum(weights, axis=-1, keepdims=True)
-    averaged = nn_dot(weights.astype(jnp.bfloat16), latent_rows) / total
-    everything = nn_dot(averaged.astype(jnp.bfloat16), value_matrix)
+    averaged = state[2] / state[1]
+    everything = nn_dot(averaged.astype(bf16), value_matrix)
     value_lane = lax.broadcasted_iota(jnp.int32, (span, H * V), 1)
-    attended = jnp.zeros((span, H * V), jnp.float32)
+    attended = jnp.zeros((span, H * V), f32)
     for h in range(H):
         attended = jnp.where(
             (value_lane >= h * V) & (value_lane < (h + 1) * V), everything[h * span:(h + 1) * span], attended)
-    attended = attended.astype(jnp.bfloat16)
+    attended = attended.astype(bf16)
     rest(3)
     columns = out_w.shape[1]
     for j in range(S):
         part = nn_dot(attended, out_all[j])
         for i in range(T):
-            part_buf[i, :, j * columns:(j + 1) * columns] = part[i * rows:(i + 1) * rows].astype(jnp.bfloat16)
+            part_buf[i, :, j * columns:(j + 1) * columns] = part[i * rows:(i + 1) * rows].astype(bf16)
     part_sent = []
     for k in range(1, T):
-        copy = pltpu.make_async_remote_copy(
-            src_ref=part_buf.at[mate(k)], dst_ref=part_all.at[k - 1], send_sem=part_send.at[k - 1],
-            recv_sem=part_recv.at[k - 1], device_id={"sp": s, "tp": mate(k)}, device_id_type=MESH)
+        copy = remote(part_buf.at[mate(k)], part_all.at[k - 1], part_send.at[k - 1], part_recv.at[k - 1], s, mate(k))
         copy.start()
         part_sent.append(copy)
-    mixed = part_buf[t].astype(jnp.float32)
+    mixed = part_buf[t].astype(f32)
     for k in range(1, T):
         part_sent[k - 1].wait_recv()
-        mixed = mixed + part_all[k - 1].astype(jnp.float32)
-    out[...] = normalize(mixed, output_gain[...]).astype(jnp.bfloat16)
-    for copy in tok_sent + raw_sent + row_sent + part_sent + [c for group in weight_sent for c in group]:
+        mixed = mixed + part_all[k - 1].astype(f32)
+    out[...] = normalize(mixed, output_gain[...]).astype(bf16)
+    for copy in tok_sent + raw_sent + row_sent + core_sent + part_sent + [c for group in weight_sent for c in group]:
         copy.wait_send()
 
 
@@ -457,6 +557,10 @@
         and key_up.shape[0] % 16 == 0
         and output_weight.shape[1] % LANES == 0
         and H * R == LANES
+        and T % 2 == 0
+        and (tokens.shape[0] * T) % 32 == 0
+        and R % 32 == 0
+        and query_down.shape[0] == LANES
         and H * N % LANES == 0
         and N == V
     )
@@ -481,43 +585,52 @@
     QW, LW = query_down.shape[1], latent_down.shape[1]
     rows, width = tokens.shape
     span = rows * T
-    h2 = R // 2
-    depth = query_down.shape[0]
-    gap = jnp.zeros((depth, LANES // 2 - h2), jnp.bfloat16)
-    packed = jnp.concatenate(
-        [query_down, rope_down[:, :h2], gap, rope_down[:, h2:], gap, latent_down], axis=1)
-    share = packed.shape[1] // T
-    down = lax.dynamic_slice_in_dim(packed, lax.axis_index("tp") * share, share, 1).T
-    q_rows = query_up.shape[0]
-    query_pack = jnp.concatenate(
-        [query_up[..., :N].reshape(q_rows, H * N),
-         query_up[..., N:].reshape(q_rows, H, 2, h2).transpose(0, 2, 1, 3).reshape(q_rows, H * R)], axis=1)
-    k_rows = key_up.shape[0]
-    kv_pack = jnp.concatenate([key_up.reshape(k_rows, H * N), value_up.reshape(k_rows, H * V)], axis=0)
+    share = (QW + LANES + LW) // T
     table = jnp.asarray(rope_tables(S * span, R, H))
     sizes = dict(S=S, T=T, H=H, N=N, V=V, R=R, QW=QW, LW=LW)
     vmem = pl.BlockSpec(memory_space=pltpu.VMEM)
     bf16 = jnp.bfloat16
     sem = pltpu.SemaphoreType.DMA
+    hbm = pl.BlockSpec(memory_space=pltpu.HBM)
+    wq = (query_up.shape[0], H * (N + R))
+    wkv = (2 * key_up.shape[0], H * N)
     return pl.pallas_call(
         functools.partial(layer_kernel, sizes),
         out_shape=jax.ShapeDtypeStruct((rows, width), bf16),
-        in_specs=[vmem] * 9 + [pl.BlockSpec(memory_space=pl.ANY)],
+        in_specs=[hbm] * 13,
         out_specs=vmem,
         scratch_shapes=[
+            pltpu.VMEM((1, span), jnp.int32),
+            pltpu.VMEM((1, QW), jnp.float32),
+            pltpu.VMEM((1, LW), jnp.float32),
+            pltpu.VMEM((1, width), jnp.float32),
+            pltpu.VMEM(tokens.shape, bf16),
+            pltpu.VMEM(query_down.shape, bf16),
+            pltpu.VMEM(latent_down.shape, bf16),
+            pltpu.VMEM(rope_down.shape[::-1], bf16),
+            pltpu.VMEM(query_up.shape, bf16),
+            pltpu.VMEM(key_up.shape, bf16),
+            pltpu.VMEM(value_up.shape, bf16),
+            pltpu.VMEM(output_weight.shape, bf16),
+            pltpu.VMEM((2, span, LANES), jnp.float32),
+            pltpu.VMEM((QW + LANES + LW, query_down.shape[0]), bf16),
+            pltpu.VMEM(wq, bf16),
+            pltpu.VMEM(wkv, bf16),
             pltpu.VMEM((T, rows, width), bf16),
-            pltpu.VMEM((S,) + down.shape, bf16),
-            pltpu.VMEM((S,) + query_pack.shape, bf16),
-            pltpu.VMEM((S,) + kv_pack.shape, bf16),
+            pltpu.VMEM((span, width), bf16),
+            pltpu.VMEM((S, share, query_down.shape[0]), bf16),
+            pltpu.VMEM((S,) + wq, bf16),
+            pltpu.VMEM((S,) + wkv, bf16),
             pltpu.VMEM((S,) + output_weight.shape, bf16),
             pltpu.VMEM((T, span, share), bf16),
             pltpu.VMEM((span, LW + LANES), bf16),
             pltpu.VMEM((S, span, LW + LANES), bf16),
             pltpu.VMEM((T, rows, width), bf16),
             pltpu.VMEM((T - 1, rows, width), bf16),
-            pltpu.VMEM((2, span, LANES), jnp.float32),
             sem((4, S - 1)),
             sem((4, S - 1)),
+            sem((S - 1,)),
+            sem((S - 1,)),
             sem((S - 1,)),
             sem((S - 1,)),
             sem((T - 1,)),
@@ -526,11 +639,11 @@
             sem((T - 1,)),
             sem((T - 1,)),
             sem((T - 1,)),
-            sem((1,)),
+            sem((13,)),
         ],
         compiler_params=pltpu.CompilerParams(
             collective_id=0, has_side_effects=True, vmem_limit_bytes=48 * 1024 * 1024),
-    )(tokens, doc_ids[:, None], down, query_pack, kv_pack, output_weight,
+    )(tokens, doc_ids[None, :], query_down, latent_down, rope_down.T, query_up, key_up, value_up, output_weight,
       query_gain[None, :], latent_gain[None, :], output_gain[None, :], table)
 
 

time: 53 us -> 53.1 us (level)
  Pallas kernels: 42.8 us -> 43.7 us
  local copies, waits for them, and re-layouts: 9.47 us -> 8.85 us
    slice x1 -> x0, local copies, waits for them, and re-layouts: 0.89 us -> none  [on_device(): query_up[..., N:].reshape(q_rows, H, 2, h2).transpose(0, 2, 1, 3)]
    pallas_call x1, Pallas kernels: 42.8 us -> 43.7 us  [on_device(): pl.pallas_call(functools.partial(layer_kernel, sizes), out_shape=jax.Shap...]
    broadcast_in_dim x1, local copies, waits for them, and re-layouts: 0.01 us -> 0.72 us  [on_device(): query_gain[None, :]]
    unnamed x29 -> x25, local copies, waits for them, and re-layouts: 8.05 us -> 8.13 us
where the time goes in v2:
time: 53.1 us; the launch traced here: 52.6 us
  Pallas kernels  43.7 us (82%)
  local copies, waits for them, and re-layouts  8.85 us (17%)
    pallas_call x1, Pallas kernels, on_device(): pl.pallas_call(functools.partial(layer_kernel, sizes), out_shape=jax.Shap...  43.7 us
    unnamed x25, local copies, waits for them, and re-layouts  8.13 us

profile of v2, /device:TPU:0, one launch (start us, length us, event | category | flops | bytes accessed | tf_op | source)
XLA Modules:
  0.0 52.6 jit_solution(9629811213940940033)
XLA Ops:
  0.0 0.0 copy-start.8
  0.0 0.0 copy-start.10
  0.0 0.0 copy-start.11
  0.0 0.7 %broadcast_in_dim.13.query_gain_in = f32[1,384]{1,0:T(1,128)S(1)} reshape(f32[384]{0:T(512)} %param.16) | data formatting | bytes 3072 | tf_op jit(solution)/shard_map/broadcast_in_dim | solution.py:647
  0.7 0.0 copy-done.8
  0.7 0.0 copy-done.10
  0.7 0.0 copy-done.11
  0.7 0.0 copy-start
  0.8 1.1 %copy-done = f32[2,768,128]{2,1,0:T(8,128)S(1)} copy-done((f32[2,768,128]{2,1,0:T(8,128)S(1)}, f32[2,768,128]{2,1,0:T(8,128)}, u32[]{:S(2)}) %copy-start) | copy-done | bytes 786456
  1.9 0.0 copy-start.1
  1.9 0.9 %copy-done.1 = bf16[128,384]{1,0:T(8,128)(2,1)S(1)} copy-done((bf16[128,384]{1,0:T(8,128)(2,1)S(1)}, bf16[128,384]{1,0:T(8,128)(2,1)}, u32[]{:S(2)}) %copy-start.1) | copy-done | bytes 98328
  2.8 0.0 copy-start.2
  2.8 0.8 %copy-done.2 = bf16[128,256]{1,0:T(8,128)(2,1)S(1)} copy-done((bf16[128,256]{1,0:T(8,128)(2,1)S(1)}, bf16[128,256]{1,0:T(8,128)(2,1)}, u32[]{:S(2)}) %copy-start.2) | copy-done | bytes 65560
  3.6 0.0 copy-start.3
  3.6 0.8 %copy-done.3 = bf16[256,128]{1,0:T(8,128)(2,1)S(1)} copy-done((bf16[256,128]{1,0:T(8,128)(2,1)S(1)}, bf16[256,128]{1,0:T(8,128)(2,1)}, u32[]{:S(2)}) %copy-start.3) | copy-done | bytes 65560
  4.5 0.0 copy-start.4
  4.5 0.8 %copy-done.4 = bf16[24,1024]{1,0:T(8,128)(2,1)S(1)} copy-done((bf16[24,1024]{1,0:T(8,128)(2,1)S(1)}, bf16[24,1024]{1,0:T(8,128)(2,1)}, u32[]{:S(2)}) %copy-start.4) | copy-done | bytes 49176
  5.3 0.0 copy-start.5
  5.3 0.8 %copy-done.5 = bf16[48,4,96]{2,1,0:T(4,128)(2,1)S(1)} copy-done((bf16[48,4,96]{2,1,0:T(4,128)(2,1)S(1)}, bf16[48,4,96]{2,1,0:T(4,128)(2,1)}, u32[]{:S(2)}) %copy-start.5) | copy-done | bytes 36888
  6.0 0.0 copy-start.6
  6.1 0.8 %copy-done.6 = bf16[32,4,64]{2,1,0:T(4,128)(2,1)S(1)} copy-done((bf16[32,4,64]{2,1,0:T(4,128)(2,1)S(1)}, bf16[32,4,64]{2,1,0:T(4,128)(2,1)}, u32[]{:S(2)}) %copy-start.6) | copy-done | bytes 16408
  6.8 0.0 copy-start.7
  6.8 0.8 %copy-done.7 = bf16[32,4,64]{2,1,0:T(4,128)(2,1)S(1)} copy-done((bf16[32,4,64]{2,1,0:T(4,128)(2,1)S(1)}, bf16[32,4,64]{2,1,0:T(4,128)(2,1)}, u32[]{:S(2)}) %copy-start.7) | copy-done | bytes 16408
  7.6 0.0 copy-start.9
  7.6 0.7 %copy-done.9 = f32[1024]{0:T(1024)S(1)} copy-done((f32[1024]{0:T(1024)S(1)}, f32[1024]{0:T(1024)}, u32[]{:S(2)}) %copy-start.9) | copy-done | bytes 4120
  8.3 43.7 %shard_map.127 = bf16[24,1024]{1,0:T(8,128)(2,1)S(1)} custom-call(bf16[24,1024]{1,0:T(8,128)(2,1)S(1)} %copy-done.4, s32[1,96]{1,0:T(1,128)S(1)} %bitcast.7, bf16[128,384]{1,0:T(8,128)(2,1)S(1)} %copy-done.1, bf16[128,256]{1,0:T(8,128)(2,1)S(1)} %copy-done.2, bf16[32,128]{1,0:T(8,128)(2,1)S(1)} %bitcast.4, bf16[48,4,96]{2,1,0:T(4,128)(2,1)S(1)} %copy-done.5, ...), custom_call_target="tpu_custom_call" | custom-call | tf_op jit(solution)/shard_map/pallas_call | solution.py:597
  51.9 0.6 %copy.15 = bf16[24,1024]{1,0:T(8,128)(2,1)} copy(bf16[24,1024]{1,0:T(8,128)(2,1)S(1)} %shard_map.127) | data formatting | bytes 98304
Async XLA Ops:
  0.0 0.7 %copy-start.8 = (bf16[128,32]{0,1:T(8,128)(2,1)S(1)}, bf16[128,32]{0,1:T(8,128)(2,1)}, u32[]{:S(2)}) copy-start(bf16[128,32]{0,1:T(8,128)(2,1)} %param.20) | copy-start | bytes 24580
  0.0 0.7 %copy-start.10 = (f32[256]{0:T(256)S(1)}, f32[256]{0:T(256)}, u32[]{:S(2)}) copy-start(f32[256]{0:T(256)} %param.19) | copy-start | bytes 3076
  0.0 0.7 %copy-start.11 = (s32[96]{0:T(128)S(1)}, s32[96]{0:T(128)}, u32[]{:S(2)}) copy-start(s32[96]{0:T(128)} %param.14) | copy-start | bytes 1156
  0.7 1.1 %copy-start = (f32[2,768,128]{2,1,0:T(8,128)S(1)}, f32[2,768,128]{2,1,0:T(8,128)}, u32[]{:S(2)}) copy-start(f32[2,768,128]{2,1,0:T(8,128)} %constant.2.clone.table) | copy-start | bytes 2359300
  1.9 0.9 %copy-start.1 = (bf16[128,384]{1,0:T(8,128)(2,1)S(1)}, bf16[128,384]{1,0:T(8,128)(2,1)}, u32[]{:S(2)}) copy-start(bf16[128,384]{1,0:T(8,128)(2,1)} %query_down.1) | copy-start | bytes 294916
  2.8 0.8 %copy-start.2 = (bf16[128,256]{1,0:T(8,128)(2,1)S(1)}, bf16[128,256]{1,0:T(8,128)(2,1)}, u32[]{:S(2)}) copy-start(bf16[128,256]{1,0:T(8,128)(2,1)} %latent_down.1) | copy-start | bytes 196612
  3.6 0.8 %copy-start.3 = (bf16[256,128]{1,0:T(8,128)(2,1)S(1)}, bf16[256,128]{1,0:T(8,128)(2,1)}, u32[]{:S(2)}) copy-start(bf16[256,128]{1,0:T(8,128)(2,1)} %out_in.1) | copy-start | bytes 196612
  4.5 0.8 %copy-start.4 = (bf16[24,1024]{1,0:T(8,128)(2,1)S(1)}, bf16[24,1024]{1,0:T(8,128)(2,1)}, u32[]{:S(2)}) copy-start(bf16[24,1024]{1,0:T(8,128)(2,1)} %tok_in.1) | copy-start | bytes 147460
  5.3 0.8 %copy-start.5 = (bf16[48,4,96]{2,1,0:T(4,128)(2,1)S(1)}, bf16[48,4,96]{2,1,0:T(4,128)(2,1)}, u32[]{:S(2)}) copy-start(bf16[48,4,96]{2,1,0:T(4,128)(2,1)} %query_up.1) | copy-start | bytes 110596
  6.0 0.8 %copy-start.6 = (bf16[32,4,64]{2,1,0:T(4,128)(2,1)S(1)}, bf16[32,4,64]{2,1,0:T(4,128)(2,1)}, u32[]{:S(2)}) copy-start(bf16[32,4,64]{2,1,0:T(4,128)(2,1)} %key_up.1) | copy-start | bytes 49156
  6.8 0.8 %copy-start.7 = (bf16[32,4,64]{2,1,0:T(4,128)(2,1)S(1)}, bf16[32,4,64]{2,1,0:T(4,128)(2,1)}, u32[]{:S(2)}) copy-start(bf16[32,4,64]{2,1,0:T(4,128)(2,1)} %value_up.1) | copy-start | bytes 49156
  7.6 0.7 %copy-start.9 = (f32[1024]{0:T(1024)S(1)}, f32[1024]{0:T(1024)}, u32[]{:S(2)}) copy-start(f32[1024]{0:T(1024)} %param.24) | copy-start | bytes 12292

commit v3 on v2

--- a/solution.py
+++ b/solution.py
@@ -642,7 +642,7 @@
             sem((13,)),
         ],
         compiler_params=pltpu.CompilerParams(
-            collective_id=0, has_side_effects=True, vmem_limit_bytes=48 * 1024 * 1024),
+            collective_id=0, has_side_effects=True, vmem_limit_bytes=67043328),
     )(tokens, doc_ids[None, :], query_down, latent_down, rope_down.T, query_up, key_up, value_up, output_weight,
       query_gain[None, :], latent_gain[None, :], output_gain[None, :], table)
 

time: 53.1 us -> 47.2 us (0.89)
  local copies, waits for them, and re-layouts: 8.85 us -> 2.67 us
  Pallas kernels: 43.7 us -> 44.3 us
    unnamed x25 -> x3, local copies, waits for them, and re-layouts: 8.13 us -> 2.1 us
    pallas_call x1, Pallas kernels: 43.7 us -> 44.3 us  [on_device(): pl.pallas_call(functools.partial(layer_kernel, sizes), out_shape=jax.Shap...]
where the time goes in v3:
time: 47.2 us; the launch traced here: 47 us
  Pallas kernels  44.3 us (94%)
  local copies, waits for them, and re-layouts  2.67 us (6%)
    pallas_call x1, Pallas kernels, on_device(): pl.pallas_call(functools.partial(layer_kernel, sizes), out_shape=jax.Shap...  44.3 us
    unnamed x3, local copies, waits for them, and re-layouts  2.1 us

profile of v3, /device:TPU:0, one launch (start us, length us, event | category | flops | bytes accessed | tf_op | source)
XLA Modules:
  0.0 47.0 jit_solution(375374514758943696)
XLA Ops:
  0.0 0.0 copy-start
  0.0 0.7 %copy-done = f32[384]{0:T(512)S(1)} copy-done((f32[384]{0:T(512)S(1)}, f32[384]{0:T(512)}, u32[]{:S(2)}) %copy-start) | copy-done | bytes 1560
  0.7 0.6 %broadcast_in_dim.13.query_gain_in = f32[1,384]{1,0:T(1,128)} reshape(f32[384]{0:T(512)S(1)} %copy-done) | data formatting | bytes 3072 | tf_op jit(solution)/shard_map/broadcast_in_dim | solution.py:647
  1.2 44.3 %shard_map.127 = bf16[24,1024]{1,0:T(8,128)(2,1)} custom-call(bf16[24,1024]{1,0:T(8,128)(2,1)} %tok_in.1, s32[1,96]{1,0:T(1,128)} %bitcast.7, bf16[128,384]{1,0:T(8,128)(2,1)} %query_down.1, bf16[128,256]{1,0:T(8,128)(2,1)} %latent_down.1, bf16[32,128]{1,0:T(8,128)(2,1)} %bitcast.4, bf16[48,4,96]{2,1,0:T(4,128)(2,1)} %query_up.1, bf16[32,4,64]{2,1,0:T(4,128)(2,1)} %key_up.1, ...), custom_call_target="tpu_custom_call" | custom-call | tf_op jit(solution)/shard_map/pallas_call | solution.py:597
  45.5 1.4 %copy.15 = bf16[24,1024]{1,0:T(8,128)(2,1)} copy(bf16[24,1024]{1,0:T(8,128)(2,1)} %shard_map.127) | data formatting | bytes 98304
Async XLA Ops:
  0.0 0.7 %copy-start = (f32[384]{0:T(512)S(1)}, f32[384]{0:T(512)}, u32[]{:S(2)}) copy-start(f32[384]{0:T(512)} %param.16) | copy-start | bytes 4612

commit v4 on v3

--- a/solution.py
+++ b/solution.py
@@ -441,7 +441,7 @@
         return x * cosine + pltpu.roll(x, LANES // 2, 1) * sine
 
     key_marks = jnp.where(is_id & (id_lane != own_id), -1.0, 0.0)
-    row_buf[:, :LW] = normalize(latent_raw, latent_gain[...]).astype(bf16)
+    row_buf[:, :LW] = normalize(latent_raw, latent_gain[...][None, :]).astype(bf16)
     row_buf[:, LW:] = jnp.where(is_id, key_marks, turn(rope_raw)).astype(bf16)
     part_rows = span // 2
     mine = pl.ds(pl.multiple_of((t % 2) * part_rows, 16), part_rows)
@@ -454,7 +454,7 @@
     relay(2)
     begin(3)
 
-    query_lat = normalize(query_raw, query_gain[...]).astype(bf16)
+    query_lat = normalize(query_raw, query_gain[...][None, :]).astype(bf16)
     rest(1)
     queries = nn_dot(query_lat, query_all[...].reshape(QW, query_pack.shape[1]))
     nope = queries[:, :H * N].astype(bf16)
@@ -491,7 +491,7 @@
     state = [peak, jnp.sum(first, axis=-1, keepdims=True), nn_dot(first.astype(bf16), row_buf[:, :LW])]
 
     def fold(blocks):
-        key_rows = jnp.concatenate([row_all[b].astype(f32) for b in blocks], axis=0).astype(bf16)
+        key_rows = jnp.concatenate([row_all[b] for b in blocks], axis=0)
         scores = block_scores(key_rows)
         peak, total, running = state
         peak_new = jnp.maximum(peak, jnp.max(scores, axis=-1, keepdims=True))
@@ -504,15 +504,18 @@
     blocks = [pass_on(row_view, row_send, row_recv, row_sent, k) for k in range(1, half)]
     for slot, block in enumerate(blocks):
         to_twin(block, slot)
-    for j in range(half):
+    landed(row_view, row_send, row_recv, half - 1)
+    to_twin(pair, half - 1)
+    blocks.append(pair)
+    for copy in core_sent:
+        copy.wait_recv()
+    fold(blocks)
+    for j in range(1, half):
         landed(row_view, row_send, row_recv, half - 1 + j)
         to_twin(pair_block(j), half - 1 + j)
-    for copy in core_sent[:half - 1]:
+    for copy in core_sent[half:]:
         copy.wait_recv()
-    fold(blocks)
-    for copy in core_sent[half - 1:]:
-        copy.wait_recv()
-    fold([pair_block(j) for j in range(half)])
+    fold([pair_block(j) for j in range(1, half)])
     relay(3)
     averaged = state[2] / state[1]
     everything = nn_dot(averaged.astype(bf16), value_matrix)
@@ -537,7 +540,7 @@
     for k in range(1, T):
         part_sent[k - 1].wait_recv()
         mixed = mixed + part_all[k - 1].astype(f32)
-    out[...] = normalize(mixed, output_gain[...]).astype(bf16)
+    out[...] = normalize(mixed, output_gain[...][None, :]).astype(bf16)
     for copy in tok_sent + raw_sent + row_sent + core_sent + part_sent + [c for group in weight_sent for c in group]:
         copy.wait_send()
 
@@ -601,9 +604,9 @@
         out_specs=vmem,
         scratch_shapes=[
             pltpu.VMEM((1, span), jnp.int32),
-            pltpu.VMEM((1, QW), jnp.float32),
-            pltpu.VMEM((1, LW), jnp.float32),
-            pltpu.VMEM((1, width), jnp.float32),
+            pltpu.VMEM((QW,), jnp.float32),
+            pltpu.VMEM((LW,), jnp.float32),
+            pltpu.VMEM((width,), jnp.float32),
             pltpu.VMEM(tokens.shape, bf16),
             pltpu.VMEM(query_down.shape, bf16),
             pltpu.VMEM(latent_down.shape, bf16),
@@ -644,7 +647,7 @@
         compiler_params=pltpu.CompilerParams(
             collective_id=0, has_side_effects=True, vmem_limit_bytes=67043328),
     )(tokens, doc_ids[None, :], query_down, latent_down, rope_down.T, query_up, key_up, value_up, output_weight,
-      query_gain[None, :], latent_gain[None, :], output_gain[None, :], table)
+      query_gain, latent_gain, output_gain, table)
 
 
 def solution(mesh):

time: 47.2 us -> 45.1 us (0.956)
  local copies, waits for them, and re-layouts: 2.67 us -> 1.42 us
  Pallas kernels: 44.3 us -> 43.5 us
    pallas_call x1, Pallas kernels: 44.3 us -> 43.5 us  [on_device(): pl.pallas_call(functools.partial(layer_kernel, sizes), out_shape=jax.Shap...]
    unnamed x3 -> x1, local copies, waits for them, and re-layouts: 2.1 us -> 1.42 us
    broadcast_in_dim x1 -> x0, local copies, waits for them, and re-layouts: 0.56 us -> none  [on_device(): query_gain[None, :]]
where the time goes in v4:
time: 45.1 us; the launch traced here: 44.9 us
  Pallas kernels  43.5 us (96%)
  local copies, waits for them, and re-layouts  1.42 us (3%)
    pallas_call x1, Pallas kernels, on_device(): pl.pallas_call(functools.partial(layer_kernel, sizes), out_shape=jax.Shap...  43.5 us
    unnamed x1, local copies, waits for them, and re-layouts  1.42 us

profile of v4, /device:TPU:0, one launch (start us, length us, event | category | flops | bytes accessed | tf_op | source)
XLA Modules:
  0.0 44.9 jit_solution(9187995643693272507)
XLA Ops:
  0.0 43.5 %shard_map.127 = bf16[24,1024]{1,0:T(8,128)(2,1)} custom-call(bf16[24,1024]{1,0:T(8,128)(2,1)} %tok_in.1, s32[1,96]{1,0:T(1,128)} %bitcast.3, bf16[128,384]{1,0:T(8,128)(2,1)} %query_down.1, bf16[128,256]{1,0:T(8,128)(2,1)} %latent_down.1, bf16[32,128]{1,0:T(8,128)(2,1)} %bitcast.2, bf16[48,4,96]{2,1,0:T(4,128)(2,1)} %query_up.1, bf16[32,4,64]{2,1,0:T(4,128)(2,1)} %key_up.1, ...), custom_call_target="tpu_custom_call" | custom-call | tf_op jit(solution)/shard_map/pallas_call | solution.py:600
  43.5 1.4 %copy.15 = bf16[24,1024]{1,0:T(8,128)(2,1)} copy(bf16[24,1024]{1,0:T(8,128)(2,1)} %shard_map.127) | data formatting | bytes 98304

commit v5 on v4

--- a/solution.py
+++ b/solution.py
@@ -509,6 +509,7 @@
     blocks.append(pair)
     for copy in core_sent:
         copy.wait_recv()
+    relay(3)
     fold(blocks)
     for j in range(1, half):
         landed(row_view, row_send, row_recv, half - 1 + j)
@@ -516,7 +517,6 @@
     for copy in core_sent[half:]:
         copy.wait_recv()
     fold([pair_block(j) for j in range(1, half)])
-    relay(3)
     averaged = state[2] / state[1]
     everything = nn_dot(averaged.astype(bf16), value_matrix)
     value_lane = lax.broadcasted_iota(jnp.int32, (span, H * V), 1)
@@ -525,23 +525,38 @@
         attended = jnp.where(
             (value_lane >= h * V) & (value_lane < (h + 1) * V), everything[h * span:(h + 1) * span], attended)
     attended = attended.astype(bf16)
+    columns = out_w.shape[1]
+    part_sent = []
+
+    def project(side):
+        for j in range(half):
+            part = nn_dot(attended, out_all[2 * j + side])
+            for i in range(T):
+                part_buf[i, side, :, j * columns:(j + 1) * columns] = part[i * rows:(i + 1) * rows].astype(bf16)
+        group = []
+        for k in range(1, T):
+            n = len(part_sent) * (T - 1) + k - 1
+            group.append(remote(
+                part_buf.at[mate(k), side], part_all.at[k - 1, side], part_send.at[n], part_recv.at[n], s, mate(k)))
+            group[-1].start()
+        part_sent.append(group)
+
+    project(s % 2)
     rest(3)
-    columns = out_w.shape[1]
-    for j in range(S):
-        part = nn_dot(attended, out_all[j])
-        for i in range(T):
-            part_buf[i, :, j * columns:(j + 1) * columns] = part[i * rows:(i + 1) * rows].astype(bf16)
-    part_sent = []
-    for k in range(1, T):
-        copy = remote(part_buf.at[mate(k)], part_all.at[k - 1], part_send.at[k - 1], part_recv.at[k - 1], s, mate(k))
-        copy.start()
-        part_sent.append(copy)
-    mixed = part_buf[t].astype(f32)
-    for k in range(1, T):
-        part_sent[k - 1].wait_recv()
-        mixed = mixed + part_all[k - 1].astype(f32)
+    project(1 - s % 2)
+    for group in part_sent:
+        for copy in group:
+            copy.wait_recv()
+    sides = []
+    for side in range(2):
+        total = part_buf[t, side].astype(f32)
+        for k in range(1, T):
+            total = total + part_all[k - 1, side].astype(f32)
+        sides.append(total)
+    mixed = jnp.concatenate(
+        [sides[j % 2][:, (j // 2) * columns:(j // 2 + 1) * columns] for j in range(S)], axis=1)
     out[...] = normalize(mixed, output_gain[...][None, :]).astype(bf16)
-    for copy in tok_sent + raw_sent + row_sent + core_sent + part_sent + [c for group in weight_sent for c in group]:
+    for copy in tok_sent + raw_sent + row_sent + core_sent + [c for group in part_sent for c in group] + [c for group in weight_sent for c in group]:
         copy.wait_send()
 
 
@@ -628,8 +643,8 @@
             pltpu.VMEM((T, span, share), bf16),
             pltpu.VMEM((span, LW + LANES), bf16),
             pltpu.VMEM((S, span, LW + LANES), bf16),
-            pltpu.VMEM((T, rows, width), bf16),
-            pltpu.VMEM((T - 1, rows, width), bf16),
+            pltpu.VMEM((T, 2, rows, width // 2), bf16),
+            pltpu.VMEM((T - 1, 2, rows, width // 2), bf16),
             sem((4, S - 1)),
             sem((4, S - 1)),
             sem((S - 1,)),
@@ -640,8 +655,8 @@
             sem((T - 1,)),
             sem((T - 1,)),
             sem((T - 1,)),
-            sem((T - 1,)),
-            sem((T - 1,)),
+            sem((2 * (T - 1),)),
+            sem((2 * (T - 1),)),
             sem((13,)),
         ],
         compiler_params=pltpu.CompilerParams(

time: 45.1 us -> 41.9 us (0.929)
  Pallas kernels: 43.5 us -> 40.3 us
    pallas_call x1, Pallas kernels: 43.5 us -> 40.3 us  [on_device(): pl.pallas_call(functools.partial(layer_kernel, sizes), out_shape=jax.Shap...]
where the time goes in v5:
time: 41.9 us; the launch traced here: 41.7 us
  Pallas kernels  40.3 us (96%)
  local copies, waits for them, and re-layouts  1.42 us (3%)
    pallas_call x1, Pallas kernels, on_device(): pl.pallas_call(functools.partial(layer_kernel, sizes), out_shape=jax.Shap...  40.3 us
    unnamed x1, local copies, waits for them, and re-layouts  1.42 us

profile of v5, /device:TPU:0, one launch (start us, length us, event | category | flops | bytes accessed | tf_op | source)
XLA Modules:
  0.0 41.7 jit_solution(11660710020814615775)
XLA Ops:
  0.0 40.3 %shard_map.127 = bf16[24,1024]{1,0:T(8,128)(2,1)} custom-call(bf16[24,1024]{1,0:T(8,128)(2,1)} %tok_in.1, s32[1,96]{1,0:T(1,128)} %bitcast.3, bf16[128,384]{1,0:T(8,128)(2,1)} %query_down.1, bf16[128,256]{1,0:T(8,128)(2,1)} %latent_down.1, bf16[32,128]{1,0:T(8,128)(2,1)} %bitcast.2, bf16[48,4,96]{2,1,0:T(4,128)(2,1)} %query_up.1, bf16[32,4,64]{2,1,0:T(4,128)(2,1)} %key_up.1, ...), custom_call_target="tpu_custom_call" | custom-call | tf_op jit(solution)/shard_map/pallas_call | solution.py:615
  40.3 1.4 %copy.15 = bf16[24,1024]{1,0:T(8,128)(2,1)} copy(bf16[24,1024]{1,0:T(8,128)(2,1)} %shard_map.127) | data formatting | bytes 98304

commit v6 on v5

--- a/solution.py
+++ b/solution.py
@@ -430,6 +430,8 @@
     id_lane = (lane - h2).astype(f32)
     is_id = (lane >= h2) & (lane < LANES // 2)
 
+    relay(1)
+    relay(2)
     for copy in raw_sent:
         copy.wait_recv()
     whole_raw = jnp.concatenate([raw_all[j].astype(f32) for j in range(T)], axis=1)
@@ -450,8 +452,6 @@
         return row_all.at[i, mine]
 
     row_sent = spread(row_buf.at[mine], row_view, row_send, row_recv)
-    relay(1)
-    relay(2)
     begin(3)
 
     query_lat = normalize(query_raw, query_gain[...][None, :]).astype(bf16)

time: 41.9 us -> 39 us (0.931)
  Pallas kernels: 40.3 us -> 37.4 us
    pallas_call x1, Pallas kernels: 40.3 us -> 37.4 us  [on_device(): pl.pallas_call(functools.partial(layer_kernel, sizes), out_shape=jax.Shap...]
where the time goes in v6:
time: 39 us; the launch traced here: 38.8 us
  Pallas kernels  37.4 us (96%)
  local copies, waits for them, and re-layouts  1.42 us (4%)
    pallas_call x1, Pallas kernels, on_device(): pl.pallas_call(functools.partial(layer_kernel, sizes), out_shape=jax.Shap...  37.4 us
    unnamed x1, local copies, waits for them, and re-layouts  1.42 us

profile of v6, /device:TPU:0, one launch (start us, length us, event | category | flops | bytes accessed | tf_op | source)
XLA Modules:
  0.0 38.8 jit_solution(11696287432194439752)
XLA Ops:
  0.0 37.4 %shard_map.127 = bf16[24,1024]{1,0:T(8,128)(2,1)} custom-call(bf16[24,1024]{1,0:T(8,128)(2,1)} %tok_in.1, s32[1,96]{1,0:T(1,128)} %bitcast.3, bf16[128,384]{1,0:T(8,128)(2,1)} %query_down.1, bf16[128,256]{1,0:T(8,128)(2,1)} %latent_down.1, bf16[32,128]{1,0:T(8,128)(2,1)} %bitcast.2, bf16[48,4,96]{2,1,0:T(4,128)(2,1)} %query_up.1, bf16[32,4,64]{2,1,0:T(4,128)(2,1)} %key_up.1, ...), custom_call_target="tpu_custom_call" | custom-call | tf_op jit(solution)/shard_map/pallas_call | solution.py:615
  37.4 1.4 %copy.15 = bf16[24,1024]{1,0:T(8,128)(2,1)} copy(bf16[24,1024]{1,0:T(8,128)(2,1)} %shard_map.127) | data formatting | bytes 98304
